TPU v7x, 32 devices: a whole 2x2x4 slice. The times are simulated.
32 devices in a mesh: ep: 8 (over z, x), tp: 4 (over y, core).
Axes of the slice: x: 2, y: 2, z: 4, core: 2. Of those that a mesh axis runs over, the one named last changes fastest.
Arguments:
- hidden_in: bfloat16 [256, 4096], P('ep'), may hold values from -6 to 6
- norm_gain: float32 [4096], replicated, may hold values from 0.1 to 1.9
- group_ids: int32 [256], P('ep'), may hold values from 0 to 1, as said below
- inner_ids: int32 [256, 4], P('ep'), may hold values from 0 to 7, as said below
- group_prob: float32 [256], P('ep'), may hold values from 0.25 to 1
- expert_prob: float32 [256, 4], P('ep'), may hold values from 0.1 to 1
- w_gate: bfloat16 [16, 4096, 1024], P('ep', None, 'tp'), may hold values from -0.09375 to 0.09375
- w_up: bfloat16 [16, 4096, 1024], P('ep', None, 'tp'), may hold values from -0.09375 to 0.09375
- w_down: bfloat16 [16, 1024, 4096], P('ep', None, 'tp'), may hold values from -0.1875 to 0.1875
Outputs:
- moe_out: bfloat16 [256, 4096], P('ep', 'tp')
Inputs may be any that keep to these rules, and one draw needn't show every extreme that they name: `group_ids`: among the 32 tokens of one index of ep no group is named by more than 16 tokens; one group is named by exactly 16 of them, and all of these name one common expert of it. `inner_ids`: each row names 4 different experts of the token's group.
All inputs are finite; a program needn't handle non-finite values.
Results may differ from a plain program's by a relative error of at most 0.0069.
Values may be sent and summed in bfloat16 or wider, within the bound.
No kernel may reach another device: no remote copies, remote signals or barrier semaphores. Data moves between devices by JAX's collectives and lax.ppermute only.
A program may use at most 64 MiB of HBM per device.

v0:
```python
import functools

import jax
import jax.numpy as jnp
from jax import lax
from jax.experimental import pallas as pl
from jax.experimental.pallas import tpu as pltpu
from jax.sharding import PartitionSpec as P


EPG = 8
EPS = 1e-06
LANES = 128
ANY = pl.BlockSpec(memory_space=pl.ANY)
BF16 = jnp.bfloat16
F32 = jnp.float32


def split3(value):
    high = value.astype(BF16)
    rest = value - high.astype(F32)
    mid = rest.astype(BF16)
    low = (rest - mid.astype(F32)).astype(BF16)
    return high, mid, low


def dispatch_kernel(*refs):
    sources, targets, sems, blocks = refs[:6], refs[-8:-2], refs[-2], refs[-1]
    sends, slots = refs[6:-9], refs[-9]
    capacity, width = sends[0].shape
    groups = len(sends)
    half = width - LANES
    core = lax.axis_index("tp") % 2
    copies = [
        pltpu.make_async_copy(source, target, sems.at[n])
        for n, (source, target) in enumerate(zip(sources, targets))
    ]
    for copy in copies:
        copy.start()
    for copy in copies:
        copy.wait()
    hidden, gain, group, inner, group_prob, expert_prob = targets
    tokens, features = hidden.shape
    group_row = group[...]
    strict = (
        lax.broadcasted_iota(jnp.int32, (tokens, tokens), 0)
        < lax.broadcasted_iota(jnp.int32, (tokens, tokens), 1)
    ).astype(BF16)
    slot = lax.broadcasted_iota(jnp.int32, (capacity, tokens), 0)
    one_hot = []
    for g in range(groups):
        member = group_row == g
        flags = jnp.broadcast_to(member.astype(F32), (capacity, tokens)).astype(BF16)
        rank = jnp.dot(flags, strict, preferred_element_type=F32).astype(jnp.int32)
        one_hot.append(((rank == slot) & member).astype(F32))
    picked = jnp.concatenate(one_hot, axis=0).astype(BF16)
    slots[...] = picked
    scaled = expert_prob[...] * group_prob[...]
    expert = lax.broadcasted_iota(jnp.int32, (EPG, tokens), 0)
    weight = jnp.zeros((EPG, tokens), F32)
    for k in range(inner.shape[0]):
        weight += jnp.where(inner[k : k + 1, :] == expert, scaled[k : k + 1, :], 0.0)
    terms = [term.astype(F32) for term in split3(weight)]
    terms.append(jnp.zeros((LANES - 3 * EPG, tokens), F32))
    table = jnp.concatenate(terms, axis=0).astype(BF16)
    rows_weight = lax.dot_general(
        picked, table, (((1,), (1,)), ((), ())), preferred_element_type=F32
    ).astype(BF16)
    wide = hidden[...].astype(F32)
    scale = lax.rsqrt(jnp.sum(wide * wide, axis=-1, keepdims=True) / features + EPS)
    start = pl.multiple_of(core * half, LANES)
    mine = hidden[:, pl.ds(start, half)].astype(F32)
    normed = (mine * scale * gain[:, pl.ds(start, half)]).astype(BF16)
    rows = jnp.dot(picked, normed, preferred_element_type=F32).astype(BF16)
    for g in range(groups):
        blocks[g, :, :half] = rows[g * capacity : (g + 1) * capacity, :]
        blocks[g, :, half:] = rows_weight[g * capacity : (g + 1) * capacity, :]
    own = lax.axis_index("ep") // (lax.axis_size("ep") // groups)
    for d in range(groups):
        sends[d][...] = blocks[(own + d) % groups]


def pack_kernel(*refs):
    out, row = refs[-1], 0
    for part in refs[:-1]:
        out[row : row + part.shape[0], :] = part[...]
        row += part.shape[0]


def first_half_kernel(rows, w_gate, w_up, partial):
    half = w_gate.shape[1] // 2
    start = pl.multiple_of(lax.axis_index("tp") % 2 * half, LANES)
    value = rows[:, :half]
    for e in range(w_gate.shape[0]):
        for m, source in enumerate((w_gate, w_up)):
            weight = source[e, pl.ds(start, half), :]
            partial[e, m] = jnp.dot(value, weight, preferred_element_type=F32)


def second_half_kernel(rows, other, partial, w_gate, w_up, act):
    experts = w_gate.shape[0]
    half = w_gate.shape[1] // 2
    start = pl.multiple_of((1 - lax.axis_index("tp") % 2) * half, LANES)
    value = other[:, :half]
    terms = rows[:, half:].astype(F32)
    owners = EPG // experts
    first = (lax.axis_index("ep") % owners) * experts
    lane = lax.broadcasted_iota(jnp.int32, terms.shape, 1)
    for e in range(experts):
        gate_weight = w_gate[e, pl.ds(start, half), :]
        up_weight = w_up[e, pl.ds(start, half), :]
        gate = partial[e, 0] + jnp.dot(value, gate_weight, preferred_element_type=F32)
        up = partial[e, 1] + jnp.dot(value, up_weight, preferred_element_type=F32)
        chosen = (lane % EPG == first + e) & (lane < 3 * EPG)
        weight = jnp.sum(jnp.where(chosen, terms, 0.0), axis=-1, keepdims=True)
        act[e] = (gate / (1.0 + jnp.exp(-gate)) * up * weight).astype(BF16)


def combine_kernel(*refs, owners):
    slots, out, parts, returned = refs[-2], refs[-1], refs[:owners], refs[owners:-2]
    groups = 1 + len(returned)
    capacity = slots.shape[0] // groups
    own = lax.axis_index("ep") // owners
    total = parts[0][:capacity, :].astype(F32)
    for part in parts[1:]:
        total += part[:capacity, :].astype(F32)
    values = jnp.concatenate([total.astype(BF16)] + [part[...] for part in returned], axis=0)
    starts = [pl.multiple_of((own + d) % groups * capacity, capacity) for d in range(groups)]
    spread = jnp.concatenate([slots[pl.ds(start, capacity), :] for start in starts], axis=0)
    out[...] = lax.dot_general(
        spread, values, (((0,), (0,)), ((), ())), preferred_element_type=F32
    ).astype(BF16)


def down_sum(acts, w_down, steps, total=None):
    tp_count = lax.axis_size("tp")
    me = lax.axis_index("tp")
    cols = acts[0].shape[2]
    for act, (shift, core) in zip(acts, steps):
        owner = (me + tp_count - 2 * shift) % tp_count
        owner = owner + core * (1 - 2 * (owner % 2))
        start = pl.multiple_of(owner * cols, LANES)
        for e in range(w_down.shape[0]):
            part = jnp.dot(act[e], w_down[e, pl.ds(start, cols), :], preferred_element_type=F32)
            total = part if total is None else total + part
    return total


def down_kernel(*refs, steps):
    acts, w_down, out = refs[: len(steps)], refs[-2], refs[-1]
    out[...] = down_sum(acts, w_down, steps)


def down_last_kernel(*refs, steps, owners):
    acts, w_down, base, outs = refs[: len(steps)], *refs[-owners - 2 : -owners], refs[-owners:]
    total = down_sum(acts, w_down, steps, base[...]).astype(BF16)
    rows = outs[0].shape[0]
    for j, out in enumerate(outs):
        out[...] = total[j * rows : (j + 1) * rows, :]


def owner_sum_kernel(*refs, owners):
    outs, parts = refs[owners:], refs[:owners]
    capacity = outs[0].shape[0]
    total = parts[0][capacity:, :].astype(F32)
    for part in parts[1:]:
        total += part[capacity:, :].astype(F32)
    total = total.astype(BF16)
    for n, out in enumerate(outs):
        out[...] = total[n * capacity : (n + 1) * capacity, :]


def kernel_call(body, out_shape, args, stream=(), scratch=(), flops=0, limit=16):
    placed = [pltpu.with_memory_space_constraint(value, pltpu.VMEM) for value in args]
    placed += [pltpu.with_memory_space_constraint(value, pltpu.HBM) for value in stream]
    return pl.pallas_call(
        body,
        out_shape=out_shape,
        in_specs=[pl.BlockSpec(memory_space=pltpu.VMEM)] * len(args) + [ANY] * len(stream),
        scratch_shapes=scratch,
        compiler_params=pltpu.CompilerParams(vmem_limit_bytes=limit * 2**20),
        cost_estimate=pl.CostEstimate(flops=flops, transcendentals=0, bytes_accessed=0),
    )(*placed)


def on_device(
    hidden_in, norm_gain, group_ids, inner_ids, group_prob, expert_prob, w_gate, w_up, w_down
):
    ep_count = lax.axis_size("ep")
    tp_count = lax.axis_size("tp")
    local_count, features, hidden_cols = w_gate.shape
    tokens = hidden_in.shape[0]
    groups = local_count * ep_count // EPG
    capacity = tokens // 2
    half = features // 2
    width = half + LANES
    shape = pltpu.VMEM
    small = (
        hidden_in,
        norm_gain[None, :],
        group_ids[None, :],
        inner_ids.T,
        group_prob[None, :],
        expert_prob.T,
    )
    owners = EPG // local_count
    *sends, slots = kernel_call(
        dispatch_kernel,
        [shape((capacity, width), BF16)] * groups + [shape((groups * capacity, tokens), BF16)],
        (),
        small,
        [pltpu.VMEM(value.shape, value.dtype) for value in small]
        + [
            pltpu.SemaphoreType.DMA((len(small),)),
            pltpu.VMEM((groups, capacity, width), BF16),
        ],
        flops=10**10,
    )

    def shift_group(value, d):
        pairs = [(s, (s + d * owners) % ep_count) for s in range(ep_count)]
        return lax.ppermute(value, "ep", pairs)

    def to_owner(value, j):
        return lax.ppermute(value, "ep", [(s, s ^ j) for s in range(ep_count)])

    def swap_cores(value):
        return lax.ppermute(value, "tp", [(t, t ^ 1) for t in range(tp_count)])

    def pack(parts):
        if len(parts) == 1:
            return parts[0]
        rows = sum(part.shape[0] for part in parts)
        return kernel_call(pack_kernel, shape((rows, width), BF16), parts)

    far_got = [shift_group(sends[d], d) for d in range(1, groups)]
    far_got = pack(far_got)
    own_parts, far_parts = [sends[0]], [far_got]
    for j in reversed(range(1, owners)):
        own_parts.insert(1, to_owner(sends[0], j))
        far_parts.insert(1, to_owner(far_got, j))
    rows = pack([part for pair in zip(own_parts, far_parts) for part in pair])
    other = swap_cores(rows)
    count = rows.shape[0]
    flops = count * half * hidden_cols * local_count * 4
    partial = kernel_call(
        first_half_kernel,
        shape((local_count, 2, count, hidden_cols), F32),
        (rows, w_gate, w_up),
        flops=flops,
    )
    act = kernel_call(
        second_half_kernel,
        shape((local_count, count, hidden_cols), BF16),
        (rows, other, partial, w_gate, w_up),
        flops=flops,
    )
    far = [
        lax.ppermute(act, "tp", [(t, (t + 2 * d) % tp_count) for t in range(tp_count)])
        for d in range(1, tp_count // 2)
    ]
    near = swap_cores(act)
    far = [value for each in far for value in (each, swap_cores(each))]
    out_cols = w_down.shape[2]
    steps = tuple((d, core) for d in range(tp_count // 2) for core in range(2))
    base = kernel_call(
        functools.partial(down_kernel, steps=steps[:2]),
        shape((count, out_cols), F32),
        (act, near, w_down),
        flops=10**8,
    )
    sums = kernel_call(
        functools.partial(down_last_kernel, steps=steps[2:], owners=owners),
        [shape((count // owners, out_cols), BF16)] * owners,
        (*far, w_down, base),
    )
    gathered = [sums[0]]
    for j in reversed(range(1, owners)):
        gathered.insert(1, to_owner(sums[j], j))
    totals = kernel_call(
        functools.partial(owner_sum_kernel, owners=owners),
        [shape((capacity, out_cols), BF16)] * (groups - 1),
        gathered,
    )
    returned = [shift_group(totals[d - 1], -d) for d in range(1, groups)]
    return kernel_call(
        functools.partial(combine_kernel, owners=owners),
        jax.ShapeDtypeStruct((tokens, out_cols), BF16),
        (*gathered, *returned, slots),
    )


def solution(mesh):
    placed = (
        P("ep", None),
        P(),
        P("ep"),
        P("ep", None),
        P("ep"),
        P("ep", None),
        P("ep", None, "tp"),
        P("ep", None, "tp"),
        P("ep", None, "tp"),
    )

    return jax.shard_map(on_device, mesh=mesh, in_specs=placed, out_specs=P("ep", "tp"), check_vma=False)
```

profile of v0, /device:TPU:0, one launch (start us, length us, event | category | flops | bytes accessed | tf_op | source)
XLA Modules:
  0.0 39.7 jit_solution(9316920888695618110)
XLA Ops:
  0.0 0.0 copy-start.1
  0.0 0.0 copy-start.2
  0.0 1.5 %shard_map.91 = (bf16[16,2176]{1,0:T(8,128)(2,1)S(1)}, bf16[16,2176]{1,0:T(8,128)(2,1)S(1)}, bf16[32,32]{1,0:T(8,128)(2,1)S(1)}) custom-call(bf16[32,4096]{1,0:T(8,128)(2,1)} %refs_0_.1, f32[1,4096]{1,0:T(1,128)} %bitcast.5, s32[1,32]{1,0:T(1,128)} %bitcast.8, s32[4,32]{1,0:T(4,128)} %bitcast.6, f32[1,32]{1,0:T(1,128)} %bitcast.9, f32[4,32]{1,0:T(4,128)} %bitcast.7), custom_call_target="tpu_custom_call" | custom-call | flops 10000000000 | tf_op jit(solution)/shard_map/pallas_call | solution.py:176
  1.5 4.1 %collective-permute-start = (bf16[16,2176]{1,0:T(8,128)(2,1)S(1)}, bf16[16,2176]{1,0:T(8,128)(2,1)S(1)}, u32[]{:S(2)}, u32[]{:S(2)}) collective-permute-start(bf16[16,2176]{1,0:T(8,128)(2,1)S(1)} %get-tuple-element.13), channel_id=1, source_target_pairs={{0,16},{4,20},{8,24},{12,28},{16,0},{20,4},{24,8},{28,12},{1,17},{... | collective-permute-start | bytes 208904 | tf_op jit(solution)/shard_map/ppermute | solution.py:222
  5.6 2.5 %collective-permute-start.5 = (bf16[16,2176]{1,0:T(8,128)(2,1)S(1)}, bf16[16,2176]{1,0:T(8,128)(2,1)S(1)}, u32[]{:S(2)}, u32[]{:S(2)}) collective-permute-start(bf16[16,2176]{1,0:T(8,128)(2,1)S(1)} %get-tuple-element.12.refs_0_), channel_id=1, source_target_pairs={{0,12},{4,8},{8,4},{12,0},{16,28},{20,24},{24,20},{28,16},{1,13},{... | collective-permute-start | bytes 208904 | tf_op jit(solution)/shard_map/ppermute | solution.py:225
  8.1 0.4 %collective-permute-start.3 = (bf16[16,2176]{1,0:T(8,128)(2,1)S(1)}, bf16[16,2176]{1,0:T(8,128)(2,1)S(1)}, u32[]{:S(2)}, u32[]{:S(2)}) collective-permute-start(bf16[16,2176]{1,0:T(8,128)(2,1)S(1)} %get-tuple-element.12.refs_0_), channel_id=1, source_target_pairs={{0,8},{4,12},{8,0},{12,4},{16,24},{20,28},{24,16},{28,20},{1,9},{5... | collective-permute-start | bytes 208904 | tf_op jit(solution)/shard_map/ppermute | solution.py:225
  8.6 0.5 %collective-permute-start.1 = (bf16[16,2176]{1,0:T(8,128)(2,1)S(1)}, bf16[16,2176]{1,0:T(8,128)(2,1)S(1)}, u32[]{:S(2)}, u32[]{:S(2)}) collective-permute-start(bf16[16,2176]{1,0:T(8,128)(2,1)S(1)} %get-tuple-element.12.refs_0_), channel_id=1, source_target_pairs={{0,4},{4,0},{8,12},{12,8},{16,20},{20,16},{24,28},{28,24},{1,5},{5... | collective-permute-start | bytes 208904 | tf_op jit(solution)/shard_map/ppermute | solution.py:225
  9.1 0.0 collective-permute-done.refs_1_
  9.1 2.5 %collective-permute-start.6 = (bf16[16,2176]{1,0:T(8,128)(2,1)S(1)}, bf16[16,2176]{1,0:T(8,128)(2,1)S(1)}, u32[]{:S(2)}, u32[]{:S(2)}) collective-permute-start(bf16[16,2176]{1,0:T(8,128)(2,1)S(1)} %collective-permute-done.refs_1_), channel_id=1, source_target_pairs={{0,12},{4,8},{8,4},{12,0},{16,28},{20,24},{24,20},{28,16},{1,13},{... | collective-permute-start | bytes 208904 | tf_op jit(solution)/shard_map/ppermute | solution.py:225
  11.6 0.6 %collective-permute-start.4 = (bf16[16,2176]{1,0:T(8,128)(2,1)S(1)}, bf16[16,2176]{1,0:T(8,128)(2,1)S(1)}, u32[]{:S(2)}, u32[]{:S(2)}) collective-permute-start(bf16[16,2176]{1,0:T(8,128)(2,1)S(1)} %collective-permute-done.refs_1_), channel_id=1, source_target_pairs={{0,8},{4,12},{8,0},{12,4},{16,24},{20,28},{24,16},{28,20},{1,9},{5... | collective-permute-start | bytes 208904 | tf_op jit(solution)/shard_map/ppermute | solution.py:225
  12.2 0.0 collective-permute-done.5.refs_6_
  12.2 1.0 %collective-permute-start.2 = (bf16[16,2176]{1,0:T(8,128)(2,1)S(1)}, bf16[16,2176]{1,0:T(8,128)(2,1)S(1)}, u32[]{:S(2)}, u32[]{:S(2)}) collective-permute-start(bf16[16,2176]{1,0:T(8,128)(2,1)S(1)} %collective-permute-done.refs_1_), channel_id=1, source_target_pairs={{0,4},{4,0},{8,12},{12,8},{16,20},{20,16},{24,28},{28,24},{1,5},{5... | collective-permute-start | bytes 208904 | tf_op jit(solution)/shard_map/ppermute | solution.py:225
  13.2 0.0 collective-permute-done.3.refs_4_
  13.2 0.7 %collective-permute-done.1.refs_2_ = bf16[16,2176]{1,0:T(8,128)(2,1)S(1)} collective-permute-done((bf16[16,2176]{1,0:T(8,128)(2,1)S(1)}, bf16[16,2176]{1,0:T(8,128)(2,1)S(1)}, u32[]{:S(2)}, u32[]{:S(2)}) %collective-permute-start.1) | collective-permute-done | bytes 69664 | tf_op jit(solution)/shard_map/ppermute | solution.py:225
  13.9 0.8 %collective-permute-done.6.refs_7_ = bf16[16,2176]{1,0:T(8,128)(2,1)S(1)} collective-permute-done((bf16[16,2176]{1,0:T(8,128)(2,1)S(1)}, bf16[16,2176]{1,0:T(8,128)(2,1)S(1)}, u32[]{:S(2)}, u32[]{:S(2)}) %collective-permute-start.6) | collective-permute-done | bytes 69664 | tf_op jit(solution)/shard_map/ppermute | solution.py:225
  14.7 1.2 %collective-permute-done.4.refs_5_ = bf16[16,2176]{1,0:T(8,128)(2,1)S(1)} collective-permute-done((bf16[16,2176]{1,0:T(8,128)(2,1)S(1)}, bf16[16,2176]{1,0:T(8,128)(2,1)S(1)}, u32[]{:S(2)}, u32[]{:S(2)}) %collective-permute-start.4) | collective-permute-done | bytes 69664 | tf_op jit(solution)/shard_map/ppermute | solution.py:225
  15.9 0.6 %collective-permute-done.2.refs_3_ = bf16[16,2176]{1,0:T(8,128)(2,1)S(1)} collective-permute-done((bf16[16,2176]{1,0:T(8,128)(2,1)S(1)}, bf16[16,2176]{1,0:T(8,128)(2,1)S(1)}, u32[]{:S(2)}, u32[]{:S(2)}) %collective-permute-start.2) | collective-permute-done | bytes 69664 | tf_op jit(solution)/shard_map/ppermute | solution.py:225
  16.5 0.1 collective-permute-start.7
  16.6 0.0 copy-done.1
  16.6 0.0 copy-done.2
  16.6 0.7 %shard_map.93.partial = f32[2,2,128,256]{3,2,1,0:T(8,128)S(1)} custom-call(bf16[128,2176]{1,0:T(8,128)(2,1)S(1)} %shard_map.92.rows, bf16[2,4096,256]{2,1,0:T(8,128)(2,1)S(1)} %copy-done.1, bf16[2,4096,256]{2,1,0:T(8,128)(2,1)S(1)} %copy-done.2), custom_call_target="tpu_custom_call" | custom-call | flops 536870912 | tf_op jit(solution)/shard_map/pallas_call | solution.py:176
  17.4 0.0 copy-start
  17.4 1.2 %collective-permute-done.7.other = bf16[128,2176]{1,0:T(8,128)(2,1)S(1)} collective-permute-done((bf16[128,2176]{1,0:T(8,128)(2,1)S(1)}, bf16[128,2176]{1,0:T(8,128)(2,1)S(1)}, u32[]{:S(2)}, u32[]{:S(2)}) %collective-permute-start.7) | collective-permute-done | bytes 557088 | tf_op jit(solution)/shard_map/ppermute | solution.py:228
  18.6 0.7 %shard_map.94.refs_0_ = bf16[2,128,256]{2,1,0:T(8,128)(2,1)S(1)} custom-call(bf16[128,2176]{1,0:T(8,128)(2,1)S(1)} %shard_map.92.rows, bf16[128,2176]{1,0:T(8,128)(2,1)S(1)} %collective-permute-done.7.other, f32[2,2,128,256]{3,2,1,0:T(8,128)S(1)} %shard_map.93.partial, bf16[2,4096,256]{2,1,0:T(8,128)(2,1)S(1)} %copy-done.1, bf16[2,4096,256]{2,1,0:T(8,128)(2,1)S(1)} %copy-done.2), custom_call_target="tpu_custom_call" | custom-call | flops 536870912 | tf_op jit(solution)/shard_map/pallas_call | solution.py:176
  19.3 1.6 %collective-permute-start.8 = (bf16[2,128,256]{2,1,0:T(8,128)(2,1)S(1)}, bf16[2,128,256]{2,1,0:T(8,128)(2,1)S(1)}, u32[]{:S(2)}, u32[]{:S(2)}) collective-permute-start(bf16[2,128,256]{2,1,0:T(8,128)(2,1)S(1)} %shard_map.94.refs_0_), channel_id=1, source_target_pairs={{0,2},{1,3},{2,0},{3,1},{4,6},{5,7},{6,4},{7,5},{8,10},{9,11},{10,... | collective-permute-start | bytes 393224 | tf_op jit(solution)/shard_map/ppermute | solution.py:259
  20.9 0.0 collective-permute-start.10
  20.9 4.0 %collective-permute-done.8.refs_0_ = bf16[2,128,256]{2,1,0:T(8,128)(2,1)S(1)} collective-permute-done((bf16[2,128,256]{2,1,0:T(8,128)(2,1)S(1)}, bf16[2,128,256]{2,1,0:T(8,128)(2,1)S(1)}, u32[]{:S(2)}, u32[]{:S(2)}) %collective-permute-start.8) | collective-permute-done | bytes 131104 | tf_op jit(solution)/shard_map/ppermute | solution.py:259
  24.9 0.0 collective-permute-start.9
  24.9 0.0 collective-permute-done.10.refs_1_
  24.9 0.0 copy-done
  24.9 0.5 %shard_map.95.refs_3_ = f32[128,1024]{1,0:T(8,128)S(1)} custom-call(bf16[2,128,256]{2,1,0:T(8,128)(2,1)S(1)} %shard_map.94.refs_0_, bf16[2,128,256]{2,1,0:T(8,128)(2,1)S(1)} %collective-permute-done.10.refs_1_, bf16[2,1024,1024]{2,1,0:T(8,128)(2,1)S(1)} %copy-done), custom_call_target="tpu_custom_call" | custom-call | flops 100000000 | tf_op jit(solution)/shard_map/pallas_call | solution.py:176
  25.4 0.9 %collective-permute-done.9.refs_1_ = bf16[2,128,256]{2,1,0:T(8,128)(2,1)S(1)} collective-permute-done((bf16[2,128,256]{2,1,0:T(8,128)(2,1)S(1)}, bf16[2,128,256]{2,1,0:T(8,128)(2,1)S(1)}, u32[]{:S(2)}, u32[]{:S(2)}) %collective-permute-start.9) | collective-permute-done | bytes 131104 | tf_op jit(solution)/shard_map/ppermute | solution.py:228
  26.3 0.4 %shard_map.96 = (bf16[32,1024]{1,0:T(8,128)(2,1)S(1)}, bf16[32,1024]{1,0:T(8,128)(2,1)S(1)}, bf16[32,1024]{1,0:T(8,128)(2,1)S(1)}, bf16[32,1024]{1,0:T(8,128)(2,1)S(1)}) custom-call(bf16[2,128,256]{2,1,0:T(8,128)(2,1)S(1)} %collective-permute-done.8.refs_0_, bf16[2,128,256]{2,1,0:T(8,128)(2,1)S(1)} %collective-permute-done.9.refs_1_, ...), custom_call_target="tpu_custom_call" | custom-call | tf_op jit(solution)/shard_map/pallas_call | solution.py:176
  26.7 1.0 %collective-permute-start.11 = (bf16[32,1024]{1,0:T(8,128)(2,1)S(1)}, bf16[32,1024]{1,0:T(8,128)(2,1)S(1)}, u32[]{:S(2)}, u32[]{:S(2)}) collective-permute-start(bf16[32,1024]{1,0:T(8,128)(2,1)S(1)} %get-tuple-element.15), channel_id=1, source_target_pairs={{0,4},{4,0},{8,12},{12,8},{16,20},{20,16},{24,28},{28,24},{1,5},{5... | collective-permute-start | bytes 196616 | tf_op jit(solution)/shard_map/ppermute | solution.py:225
  27.8 1.0 %collective-permute-start.12 = (bf16[32,1024]{1,0:T(8,128)(2,1)S(1)}, bf16[32,1024]{1,0:T(8,128)(2,1)S(1)}, u32[]{:S(2)}, u32[]{:S(2)}) collective-permute-start(bf16[32,1024]{1,0:T(8,128)(2,1)S(1)} %get-tuple-element.16), channel_id=1, source_target_pairs={{0,8},{4,12},{8,0},{12,4},{16,24},{20,28},{24,16},{28,20},{1,9},{5... | collective-permute-start | bytes 196616 | tf_op jit(solution)/shard_map/ppermute | solution.py:225
  28.8 1.5 %collective-permute-start.13 = (bf16[32,1024]{1,0:T(8,128)(2,1)S(1)}, bf16[32,1024]{1,0:T(8,128)(2,1)S(1)}, u32[]{:S(2)}, u32[]{:S(2)}) collective-permute-start(bf16[32,1024]{1,0:T(8,128)(2,1)S(1)} %get-tuple-element.17), channel_id=1, source_target_pairs={{0,12},{4,8},{8,4},{12,0},{16,28},{20,24},{24,20},{28,16},{1,13},{... | collective-permute-start | bytes 196616 | tf_op jit(solution)/shard_map/ppermute | solution.py:225
  30.3 0.8 %collective-permute-done.11.refs_1_ = bf16[32,1024]{1,0:T(8,128)(2,1)S(1)} collective-permute-done((bf16[32,1024]{1,0:T(8,128)(2,1)S(1)}, bf16[32,1024]{1,0:T(8,128)(2,1)S(1)}, u32[]{:S(2)}, u32[]{:S(2)}) %collective-permute-start.11) | collective-permute-done | bytes 65568 | tf_op jit(solution)/shard_map/ppermute | solution.py:225
  31.1 1.1 %collective-permute-done.12.refs_2_ = bf16[32,1024]{1,0:T(8,128)(2,1)S(1)} collective-permute-done((bf16[32,1024]{1,0:T(8,128)(2,1)S(1)}, bf16[32,1024]{1,0:T(8,128)(2,1)S(1)}, u32[]{:S(2)}, u32[]{:S(2)}) %collective-permute-start.12) | collective-permute-done | bytes 65568 | tf_op jit(solution)/shard_map/ppermute | solution.py:225
  32.2 1.8 %collective-permute-done.13.refs_3_ = bf16[32,1024]{1,0:T(8,128)(2,1)S(1)} collective-permute-done((bf16[32,1024]{1,0:T(8,128)(2,1)S(1)}, bf16[32,1024]{1,0:T(8,128)(2,1)S(1)}, u32[]{:S(2)}, u32[]{:S(2)}) %collective-permute-start.13) | collective-permute-done | bytes 65568 | tf_op jit(solution)/shard_map/ppermute | solution.py:225
  34.0 2.9 %collective-permute-start.14 = (bf16[16,1024]{1,0:T(8,128)(2,1)S(1)}, bf16[16,1024]{1,0:T(8,128)(2,1)S(1)}, u32[]{:S(2)}, u32[]{:S(2)}) collective-permute-start(bf16[16,1024]{1,0:T(8,128)(2,1)S(1)} %shard_map.97), channel_id=1, source_target_pairs={{0,16},{4,20},{8,24},{12,28},{16,0},{20,4},{24,8},{28,12},{1,17},{... | collective-permute-start | bytes 98312 | tf_op jit(solution)/shard_map/ppermute | solution.py:222
  36.9 2.0 %collective-permute-done.14.refs_4_ = bf16[16,1024]{1,0:T(8,128)(2,1)S(1)} collective-permute-done((bf16[16,1024]{1,0:T(8,128)(2,1)S(1)}, bf16[16,1024]{1,0:T(8,128)(2,1)S(1)}, u32[]{:S(2)}, u32[]{:S(2)}) %collective-permute-start.14) | collective-permute-done | bytes 32800 | tf_op jit(solution)/shard_map/ppermute | solution.py:222
  38.9 0.8 %shard_map.98 = bf16[32,1024]{1,0:T(8,128)(2,1)} custom-call(bf16[32,1024]{1,0:T(8,128)(2,1)S(1)} %get-tuple-element.14.refs_0_, bf16[32,1024]{1,0:T(8,128)(2,1)S(1)} %collective-permute-done.11.refs_1_, bf16[32,1024]{1,0:T(8,128)(2,1)S(1)} %collective-permute-done.12.refs_2_, bf16[32,1024]{1,0:T(8,128)(2,1)S(1)} %collective-permute-done.13.refs_3_, ...), custom_call_target="tpu_custom_call" | custom-call | tf_op jit(solution)/shard_map/pallas_call | solution.py:176
  (2 shorter events, 0.1 us)
Async XLA Ops:
  0.0 16.6 %copy-start.1 = (bf16[2,4096,256]{2,1,0:T(8,128)(2,1)S(1)}, bf16[2,4096,256]{2,1,0:T(8,128)(2,1)}, u32[]{:S(2)}) copy-start(bf16[2,4096,256]{2,1,0:T(8,128)(2,1)} %w_gate.3) | copy-start | bytes 12582916
  0.0 16.6 %copy-start.2 = (bf16[2,4096,256]{2,1,0:T(8,128)(2,1)S(1)}, bf16[2,4096,256]{2,1,0:T(8,128)(2,1)}, u32[]{:S(2)}) copy-start(bf16[2,4096,256]{2,1,0:T(8,128)(2,1)} %w_up.3) | copy-start | bytes 12582916
  1.5 7.6 %collective-permute-start = (bf16[16,2176]{1,0:T(8,128)(2,1)S(1)}, bf16[16,2176]{1,0:T(8,128)(2,1)S(1)}, u32[]{:S(2)}, u32[]{:S(2)}) collective-permute-start(bf16[16,2176]{1,0:T(8,128)(2,1)S(1)} %get-tuple-element.13), channel_id=1, source_target_pairs={{0,16},{4,20},{8,24},{12,28},{16,0},{20,4},{24,8},{28,12},{1,17},{... | collective-permute-start | bytes 208904 | tf_op jit(solution)/shard_map/ppermute | solution.py:222
  5.6 6.6 %collective-permute-start.5 = (bf16[16,2176]{1,0:T(8,128)(2,1)S(1)}, bf16[16,2176]{1,0:T(8,128)(2,1)S(1)}, u32[]{:S(2)}, u32[]{:S(2)}) collective-permute-start(bf16[16,2176]{1,0:T(8,128)(2,1)S(1)} %get-tuple-element.12.refs_0_), channel_id=1, source_target_pairs={{0,12},{4,8},{8,4},{12,0},{16,28},{20,24},{24,20},{28,16},{1,13},{... | collective-permute-start | bytes 208904 | tf_op jit(solution)/shard_map/ppermute | solution.py:225
  8.1 5.1 %collective-permute-start.3 = (bf16[16,2176]{1,0:T(8,128)(2,1)S(1)}, bf16[16,2176]{1,0:T(8,128)(2,1)S(1)}, u32[]{:S(2)}, u32[]{:S(2)}) collective-permute-start(bf16[16,2176]{1,0:T(8,128)(2,1)S(1)} %get-tuple-element.12.refs_0_), channel_id=1, source_target_pairs={{0,8},{4,12},{8,0},{12,4},{16,24},{20,28},{24,16},{28,20},{1,9},{5... | collective-permute-start | bytes 208904 | tf_op jit(solution)/shard_map/ppermute | solution.py:225
  8.6 5.3 %collective-permute-start.1 = (bf16[16,2176]{1,0:T(8,128)(2,1)S(1)}, bf16[16,2176]{1,0:T(8,128)(2,1)S(1)}, u32[]{:S(2)}, u32[]{:S(2)}) collective-permute-start(bf16[16,2176]{1,0:T(8,128)(2,1)S(1)} %get-tuple-element.12.refs_0_), channel_id=1, source_target_pairs={{0,4},{4,0},{8,12},{12,8},{16,20},{20,16},{24,28},{28,24},{1,5},{5... | collective-permute-start | bytes 208904 | tf_op jit(solution)/shard_map/ppermute | solution.py:225
  9.1 5.6 %collective-permute-start.6 = (bf16[16,2176]{1,0:T(8,128)(2,1)S(1)}, bf16[16,2176]{1,0:T(8,128)(2,1)S(1)}, u32[]{:S(2)}, u32[]{:S(2)}) collective-permute-start(bf16[16,2176]{1,0:T(8,128)(2,1)S(1)} %collective-permute-done.refs_1_), channel_id=1, source_target_pairs={{0,12},{4,8},{8,4},{12,0},{16,28},{20,24},{24,20},{28,16},{1,13},{... | collective-permute-start | bytes 208904 | tf_op jit(solution)/shard_map/ppermute | solution.py:225
  11.6 4.3 %collective-permute-start.4 = (bf16[16,2176]{1,0:T(8,128)(2,1)S(1)}, bf16[16,2176]{1,0:T(8,128)(2,1)S(1)}, u32[]{:S(2)}, u32[]{:S(2)}) collective-permute-start(bf16[16,2176]{1,0:T(8,128)(2,1)S(1)} %collective-permute-done.refs_1_), channel_id=1, source_target_pairs={{0,8},{4,12},{8,0},{12,4},{16,24},{20,28},{24,16},{28,20},{1,9},{5... | collective-permute-start | bytes 208904 | tf_op jit(solution)/shard_map/ppermute | solution.py:225
  12.2 4.3 %collective-permute-start.2 = (bf16[16,2176]{1,0:T(8,128)(2,1)S(1)}, bf16[16,2176]{1,0:T(8,128)(2,1)S(1)}, u32[]{:S(2)}, u32[]{:S(2)}) collective-permute-start(bf16[16,2176]{1,0:T(8,128)(2,1)S(1)} %collective-permute-done.refs_1_), channel_id=1, source_target_pairs={{0,4},{4,0},{8,12},{12,8},{16,20},{20,16},{24,28},{28,24},{1,5},{5... | collective-permute-start | bytes 208904 | tf_op jit(solution)/shard_map/ppermute | solution.py:225
  16.5 2.0 %collective-permute-start.7 = (bf16[128,2176]{1,0:T(8,128)(2,1)S(1)}, bf16[128,2176]{1,0:T(8,128)(2,1)S(1)}, u32[]{:S(2)}, u32[]{:S(2)}) collective-permute-start(bf16[128,2176]{1,0:T(8,128)(2,1)S(1)} %shard_map.92.rows), channel_id=1, source_target_pairs={{0,1},{1,0},{2,3},{3,2},{4,5},{5,4},{6,7},{7,6},{8,9},{9,8},{10,11... | collective-permute-start | bytes 1671176 | tf_op jit(solution)/shard_map/ppermute | solution.py:228
  17.4 7.6 %copy-start = (bf16[2,1024,1024]{2,1,0:T(8,128)(2,1)S(1)}, bf16[2,1024,1024]{2,1,0:T(8,128)(2,1)}, u32[]{:S(2)}) copy-start(bf16[2,1024,1024]{2,1,0:T(8,128)(2,1)} %refs_2_.3) | copy-start | bytes 12582916
  19.3 5.6 %collective-permute-start.8 = (bf16[2,128,256]{2,1,0:T(8,128)(2,1)S(1)}, bf16[2,128,256]{2,1,0:T(8,128)(2,1)S(1)}, u32[]{:S(2)}, u32[]{:S(2)}) collective-permute-start(bf16[2,128,256]{2,1,0:T(8,128)(2,1)S(1)} %shard_map.94.refs_0_), channel_id=1, source_target_pairs={{0,2},{1,3},{2,0},{3,1},{4,6},{5,7},{6,4},{7,5},{8,10},{9,11},{10,... | collective-permute-start | bytes 393224 | tf_op jit(solution)/shard_map/ppermute | solution.py:259
  20.9 4.0 %collective-permute-start.10 = (bf16[2,128,256]{2,1,0:T(8,128)(2,1)S(1)}, bf16[2,128,256]{2,1,0:T(8,128)(2,1)S(1)}, u32[]{:S(2)}, u32[]{:S(2)}) collective-permute-start(bf16[2,128,256]{2,1,0:T(8,128)(2,1)S(1)} %shard_map.94.refs_0_), channel_id=1, source_target_pairs={{0,1},{1,0},{2,3},{3,2},{4,5},{5,4},{6,7},{7,6},{8,9},{9,8},{10,11... | collective-permute-start | bytes 393224 | tf_op jit(solution)/shard_map/ppermute | solution.py:228
  24.9 1.3 %collective-permute-start.9 = (bf16[2,128,256]{2,1,0:T(8,128)(2,1)S(1)}, bf16[2,128,256]{2,1,0:T(8,128)(2,1)S(1)}, u32[]{:S(2)}, u32[]{:S(2)}) collective-permute-start(bf16[2,128,256]{2,1,0:T(8,128)(2,1)S(1)} %collective-permute-done.8.refs_0_), channel_id=1, source_target_pairs={{0,1},{1,0},{2,3},{3,2},{4,5},{5,4},{6,7},{7,6},{8,9},{9,8},{10,11... | collective-permute-start | bytes 393224 | tf_op jit(solution)/shard_map/ppermute | solution.py:228
  26.7 4.3 %collective-permute-start.11 = (bf16[32,1024]{1,0:T(8,128)(2,1)S(1)}, bf16[32,1024]{1,0:T(8,128)(2,1)S(1)}, u32[]{:S(2)}, u32[]{:S(2)}) collective-permute-start(bf16[32,1024]{1,0:T(8,128)(2,1)S(1)} %get-tuple-element.15), channel_id=1, source_target_pairs={{0,4},{4,0},{8,12},{12,8},{16,20},{20,16},{24,28},{28,24},{1,5},{5... | collective-permute-start | bytes 196616 | tf_op jit(solution)/shard_map/ppermute | solution.py:225
  27.8 4.4 %collective-permute-start.12 = (bf16[32,1024]{1,0:T(8,128)(2,1)S(1)}, bf16[32,1024]{1,0:T(8,128)(2,1)S(1)}, u32[]{:S(2)}, u32[]{:S(2)}) collective-permute-start(bf16[32,1024]{1,0:T(8,128)(2,1)S(1)} %get-tuple-element.16), channel_id=1, source_target_pairs={{0,8},{4,12},{8,0},{12,4},{16,24},{20,28},{24,16},{28,20},{1,9},{5... | collective-permute-start | bytes 196616 | tf_op jit(solution)/shard_map/ppermute | solution.py:225
  28.8 5.2 %collective-permute-start.13 = (bf16[32,1024]{1,0:T(8,128)(2,1)S(1)}, bf16[32,1024]{1,0:T(8,128)(2,1)S(1)}, u32[]{:S(2)}, u32[]{:S(2)}) collective-permute-start(bf16[32,1024]{1,0:T(8,128)(2,1)S(1)} %get-tuple-element.17), channel_id=1, source_target_pairs={{0,12},{4,8},{8,4},{12,0},{16,28},{20,24},{24,20},{28,16},{1,13},{... | collective-permute-start | bytes 196616 | tf_op jit(solution)/shard_map/ppermute | solution.py:225
  34.0 4.9 %collective-permute-start.14 = (bf16[16,1024]{1,0:T(8,128)(2,1)S(1)}, bf16[16,1024]{1,0:T(8,128)(2,1)S(1)}, u32[]{:S(2)}, u32[]{:S(2)}) collective-permute-start(bf16[16,1024]{1,0:T(8,128)(2,1)S(1)} %shard_map.97), channel_id=1, source_target_pairs={{0,16},{4,20},{8,24},{12,28},{16,0},{20,4},{24,8},{28,12},{1,17},{... | collective-permute-start | bytes 98312 | tf_op jit(solution)/shard_map/ppermute | solution.py:222
where the time goes:
time: 39.8 us; the launch traced here: 39.7 us
  starting transfers between devices  19.7 us (49%)
  waiting for transfers between devices  15.1 us (38%)
  Pallas kernels  4.75 us (12%)
    ppermute x9, starting transfers between devices, to_owner(): return lax.ppermute(value, 'ep', [(s, s ^ j) for s in range(ep_count)])  11.1 us
    ppermute x9, waiting for transfers between devices, to_owner(): return lax.ppermute(value, 'ep', [(s, s ^ j) for s in range(ep_count)])  7.01 us
    ppermute x2, starting transfers between devices, shift_group(): return lax.ppermute(value, 'ep', pairs)  7 us
    pallas_call x8, Pallas kernels, kernel_call(): pl.pallas_call(body, out_shape=out_shape, in_specs=[pl.BlockSpec(memory_s...  4.75 us
    ppermute x1, waiting for transfers between devices, on_device(): lax.ppermute(act, 'tp', [(t, (t + 2 * d) % tp_count) for t in range(tp_co...  4.02 us
    ppermute x3, waiting for transfers between devices, swap_cores(): return lax.ppermute(value, 'tp', [(t, t ^ 1) for t in range(tp_count)])  2.06 us
    ppermute x2, waiting for transfers between devices, shift_group(): return lax.ppermute(value, 'ep', pairs)  2.01 us
    ppermute x1, starting transfers between devices, on_device(): lax.ppermute(act, 'tp', [(t, (t + 2 * d) % tp_count) for t in range(tp_co...  1.58 us
  transfers between devices with their start and end apart: 15, of which 11 were waited for; matrix products, arithmetic and copies ran while one was open for 0% of the time, Pallas kernels for 3%

commit v1 on v0

--- a/solution.py
+++ b/solution.py
@@ -97,11 +97,11 @@
             partial[e, m] = jnp.dot(value, weight, preferred_element_type=F32)
 
 
-def second_half_kernel(rows, other, partial, w_gate, w_up, act):
+def second_half_kernel(rows, near, far, partial, w_gate, w_up, act):
     experts = w_gate.shape[0]
     half = w_gate.shape[1] // 2
     start = pl.multiple_of((1 - lax.axis_index("tp") % 2) * half, LANES)
-    value = other[:, :half]
+    value = jnp.concatenate([near[:, :half], far[:, :half]], axis=0)
     terms = rows[:, half:].astype(F32)
     owners = EPG // experts
     first = (lax.axis_index("ep") % owners) * experts
@@ -151,12 +151,14 @@
     out[...] = down_sum(acts, w_down, steps)
 
 
-def down_last_kernel(*refs, steps, owners):
+def down_last_kernel(*refs, steps, owners, capacity):
     acts, w_down, base, outs = refs[: len(steps)], *refs[-owners - 2 : -owners], refs[-owners:]
     total = down_sum(acts, w_down, steps, base[...]).astype(BF16)
-    rows = outs[0].shape[0]
+    far = outs[0].shape[0] - capacity
     for j, out in enumerate(outs):
-        out[...] = total[j * rows : (j + 1) * rows, :]
+        out[:capacity, :] = total[j * capacity : (j + 1) * capacity, :]
+        start = owners * capacity + j * far
+        out[capacity:, :] = total[start : start + far, :]
 
 
 def owner_sum_kernel(*refs, owners):
@@ -239,8 +241,11 @@
     for j in reversed(range(1, owners)):
         own_parts.insert(1, to_owner(sends[0], j))
         far_parts.insert(1, to_owner(far_got, j))
-    rows = pack([part for pair in zip(own_parts, far_parts) for part in pair])
-    other = swap_cores(rows)
+    near_rows = pack(own_parts)
+    near_other = swap_cores(near_rows)
+    far_rows = pack(far_parts)
+    far_other = swap_cores(far_rows)
+    rows = pack([near_rows, far_rows])
     count = rows.shape[0]
     flops = count * half * hidden_cols * local_count * 4
     partial = kernel_call(
@@ -252,7 +257,7 @@
     act = kernel_call(
         second_half_kernel,
         shape((local_count, count, hidden_cols), BF16),
-        (rows, other, partial, w_gate, w_up),
+        (rows, near_other, far_other, partial, w_gate, w_up),
         flops=flops,
     )
     far = [
@@ -270,7 +275,9 @@
         flops=10**8,
     )
     sums = kernel_call(
-        functools.partial(down_last_kernel, steps=steps[2:], owners=owners),
+        functools.partial(
+            down_last_kernel, steps=steps[2:], owners=owners, capacity=capacity
+        ),
         [shape((count // owners, out_cols), BF16)] * owners,
         (*far, w_down, base),
     )

time: 39.8 us -> 39.4 us (0.990)
  waiting for transfers between devices: 15.1 us -> 14.5 us
    ppermute x3 -> x4, waiting for transfers between devices: 2.06 us -> 1.61 us  [swap_cores(): return lax.ppermute(value, 'tp', [(t, t ^ 1) for t in range(tp_count)])]
    pallas_call x8 -> x10, Pallas kernels: 4.75 us -> 4.79 us  [kernel_call(): pl.pallas_call(body, out_shape=out_shape, in_specs=[pl.BlockSpec(memory_s...]
  transfers between devices with their start and end apart: 15 -> 16, of which waited for: 11 -> 11; matrix products, arithmetic and copies ran while one was open for 0% -> 0% of each run, Pallas kernels for 3% -> 3%
where the time goes in v1:
time: 39.4 us; the launch traced here: 39.3 us
  starting transfers between devices  19.8 us (50%)
  waiting for transfers between devices  14.5 us (37%)
  Pallas kernels  4.79 us (12%)
    ppermute x9, starting transfers between devices, to_owner(): return lax.ppermute(value, 'ep', [(s, s ^ j) for s in range(ep_count)])  11.1 us
    ppermute x2, starting transfers between devices, shift_group(): return lax.ppermute(value, 'ep', pairs)  7 us
    ppermute x9, waiting for transfers between devices, to_owner(): return lax.ppermute(value, 'ep', [(s, s ^ j) for s in range(ep_count)])  6.9 us
    pallas_call x10, Pallas kernels, kernel_call(): pl.pallas_call(body, out_shape=out_shape, in_specs=[pl.BlockSpec(memory_s...  4.79 us
    ppermute x1, waiting for transfers between devices, on_device(): lax.ppermute(act, 'tp', [(t, (t + 2 * d) % tp_count) for t in range(tp_co...  4.02 us
    ppermute x2, waiting for transfers between devices, shift_group(): return lax.ppermute(value, 'ep', pairs)  2.01 us
    ppermute x4, waiting for transfers between devices, swap_cores(): return lax.ppermute(value, 'tp', [(t, t ^ 1) for t in range(tp_count)])  1.61 us
    ppermute x1, starting transfers between devices, on_device(): lax.ppermute(act, 'tp', [(t, (t + 2 * d) % tp_count) for t in range(tp_co...  1.58 us
  transfers between devices with their start and end apart: 16, of which 11 were waited for; matrix products, arithmetic and copies ran while one was open for 0% of the time, Pallas kernels for 3%

profile of v1, /device:TPU:0, one launch (start us, length us, event | category | flops | bytes accessed | tf_op | source)
XLA Modules:
  0.0 39.3 jit_solution(12426561395940894058)
XLA Ops:
  0.0 0.0 copy-start.1
  0.0 0.0 copy-start.2
  0.0 1.5 %shard_map.91 = (bf16[16,2176]{1,0:T(8,128)(2,1)S(1)}, bf16[16,2176]{1,0:T(8,128)(2,1)S(1)}, bf16[32,32]{1,0:T(8,128)(2,1)S(1)}) custom-call(bf16[32,4096]{1,0:T(8,128)(2,1)} %refs_0_.1, f32[1,4096]{1,0:T(1,128)} %bitcast.5, s32[1,32]{1,0:T(1,128)} %bitcast.8, s32[4,32]{1,0:T(4,128)} %bitcast.6, f32[1,32]{1,0:T(1,128)} %bitcast.9, f32[4,32]{1,0:T(4,128)} %bitcast.7), custom_call_target="tpu_custom_call" | custom-call | flops 10000000000 | tf_op jit(solution)/shard_map/pallas_call | solution.py:178
  1.5 4.1 %collective-permute-start.3 = (bf16[16,2176]{1,0:T(8,128)(2,1)S(1)}, bf16[16,2176]{1,0:T(8,128)(2,1)S(1)}, u32[]{:S(2)}, u32[]{:S(2)}) collective-permute-start(bf16[16,2176]{1,0:T(8,128)(2,1)S(1)} %get-tuple-element.13), channel_id=1, source_target_pairs={{0,16},{4,20},{8,24},{12,28},{16,0},{20,4},{24,8},{28,12},{1,17},{... | collective-permute-start | bytes 208904 | tf_op jit(solution)/shard_map/ppermute | solution.py:224
  5.6 2.5 %collective-permute-start.2 = (bf16[16,2176]{1,0:T(8,128)(2,1)S(1)}, bf16[16,2176]{1,0:T(8,128)(2,1)S(1)}, u32[]{:S(2)}, u32[]{:S(2)}) collective-permute-start(bf16[16,2176]{1,0:T(8,128)(2,1)S(1)} %get-tuple-element.12.refs_0_), channel_id=1, source_target_pairs={{0,12},{4,8},{8,4},{12,0},{16,28},{20,24},{24,20},{28,16},{1,13},{... | collective-permute-start | bytes 208904 | tf_op jit(solution)/shard_map/ppermute | solution.py:227
  8.1 0.4 %collective-permute-start.1 = (bf16[16,2176]{1,0:T(8,128)(2,1)S(1)}, bf16[16,2176]{1,0:T(8,128)(2,1)S(1)}, u32[]{:S(2)}, u32[]{:S(2)}) collective-permute-start(bf16[16,2176]{1,0:T(8,128)(2,1)S(1)} %get-tuple-element.12.refs_0_), channel_id=1, source_target_pairs={{0,8},{4,12},{8,0},{12,4},{16,24},{20,28},{24,16},{28,20},{1,9},{5... | collective-permute-start | bytes 208904 | tf_op jit(solution)/shard_map/ppermute | solution.py:227
  8.6 0.5 %collective-permute-start = (bf16[16,2176]{1,0:T(8,128)(2,1)S(1)}, bf16[16,2176]{1,0:T(8,128)(2,1)S(1)}, u32[]{:S(2)}, u32[]{:S(2)}) collective-permute-start(bf16[16,2176]{1,0:T(8,128)(2,1)S(1)} %get-tuple-element.12.refs_0_), channel_id=1, source_target_pairs={{0,4},{4,0},{8,12},{12,8},{16,20},{20,16},{24,28},{28,24},{1,5},{5... | collective-permute-start | bytes 208904 | tf_op jit(solution)/shard_map/ppermute | solution.py:227
  9.1 0.0 collective-permute-done.3.refs_0_
  9.1 2.5 %collective-permute-start.6 = (bf16[16,2176]{1,0:T(8,128)(2,1)S(1)}, bf16[16,2176]{1,0:T(8,128)(2,1)S(1)}, u32[]{:S(2)}, u32[]{:S(2)}) collective-permute-start(bf16[16,2176]{1,0:T(8,128)(2,1)S(1)} %collective-permute-done.3.refs_0_), channel_id=1, source_target_pairs={{0,12},{4,8},{8,4},{12,0},{16,28},{20,24},{24,20},{28,16},{1,13},{... | collective-permute-start | bytes 208904 | tf_op jit(solution)/shard_map/ppermute | solution.py:227
  11.6 0.6 %collective-permute-start.5 = (bf16[16,2176]{1,0:T(8,128)(2,1)S(1)}, bf16[16,2176]{1,0:T(8,128)(2,1)S(1)}, u32[]{:S(2)}, u32[]{:S(2)}) collective-permute-start(bf16[16,2176]{1,0:T(8,128)(2,1)S(1)} %collective-permute-done.3.refs_0_), channel_id=1, source_target_pairs={{0,8},{4,12},{8,0},{12,4},{16,24},{20,28},{24,16},{28,20},{1,9},{5... | collective-permute-start | bytes 208904 | tf_op jit(solution)/shard_map/ppermute | solution.py:227
  12.2 0.0 collective-permute-done.2.refs_3_
  12.2 1.0 %collective-permute-start.4 = (bf16[16,2176]{1,0:T(8,128)(2,1)S(1)}, bf16[16,2176]{1,0:T(8,128)(2,1)S(1)}, u32[]{:S(2)}, u32[]{:S(2)}) collective-permute-start(bf16[16,2176]{1,0:T(8,128)(2,1)S(1)} %collective-permute-done.3.refs_0_), channel_id=1, source_target_pairs={{0,4},{4,0},{8,12},{12,8},{16,20},{20,16},{24,28},{28,24},{1,5},{5... | collective-permute-start | bytes 208904 | tf_op jit(solution)/shard_map/ppermute | solution.py:227
  13.2 0.0 collective-permute-done.1.refs_2_
  13.2 0.7 %collective-permute-done.refs_1_ = bf16[16,2176]{1,0:T(8,128)(2,1)S(1)} collective-permute-done((bf16[16,2176]{1,0:T(8,128)(2,1)S(1)}, bf16[16,2176]{1,0:T(8,128)(2,1)S(1)}, u32[]{:S(2)}, u32[]{:S(2)}) %collective-permute-start) | collective-permute-done | bytes 69664 | tf_op jit(solution)/shard_map/ppermute | solution.py:227
  13.9 0.1 collective-permute-start.7
  14.0 0.7 %collective-permute-done.6.refs_3_ = bf16[16,2176]{1,0:T(8,128)(2,1)S(1)} collective-permute-done((bf16[16,2176]{1,0:T(8,128)(2,1)S(1)}, bf16[16,2176]{1,0:T(8,128)(2,1)S(1)}, u32[]{:S(2)}, u32[]{:S(2)}) %collective-permute-start.6) | collective-permute-done | bytes 69664 | tf_op jit(solution)/shard_map/ppermute | solution.py:227
  14.7 1.2 %collective-permute-done.5.refs_2_ = bf16[16,2176]{1,0:T(8,128)(2,1)S(1)} collective-permute-done((bf16[16,2176]{1,0:T(8,128)(2,1)S(1)}, bf16[16,2176]{1,0:T(8,128)(2,1)S(1)}, u32[]{:S(2)}, u32[]{:S(2)}) %collective-permute-start.5) | collective-permute-done | bytes 69664 | tf_op jit(solution)/shard_map/ppermute | solution.py:227
  15.9 0.6 %collective-permute-done.4.refs_1_ = bf16[16,2176]{1,0:T(8,128)(2,1)S(1)} collective-permute-done((bf16[16,2176]{1,0:T(8,128)(2,1)S(1)}, bf16[16,2176]{1,0:T(8,128)(2,1)S(1)}, u32[]{:S(2)}, u32[]{:S(2)}) %collective-permute-start.4) | collective-permute-done | bytes 69664 | tf_op jit(solution)/shard_map/ppermute | solution.py:227
  16.5 0.1 collective-permute-start.8
  16.7 0.0 copy-done.1
  16.7 0.0 copy-done.2
  16.7 0.7 %shard_map.95.partial = f32[2,2,128,256]{3,2,1,0:T(8,128)S(1)} custom-call(bf16[128,2176]{1,0:T(8,128)(2,1)S(1)} %shard_map.94.rows, bf16[2,4096,256]{2,1,0:T(8,128)(2,1)S(1)} %copy-done.1, bf16[2,4096,256]{2,1,0:T(8,128)(2,1)S(1)} %copy-done.2), custom_call_target="tpu_custom_call" | custom-call | flops 536870912 | tf_op jit(solution)/shard_map/pallas_call | solution.py:178
  17.4 0.0 copy-start
  17.4 0.0 collective-permute-done.7.near
  17.4 0.7 %collective-permute-done.8.far = bf16[64,2176]{1,0:T(8,128)(2,1)S(1)} collective-permute-done((bf16[64,2176]{1,0:T(8,128)(2,1)S(1)}, bf16[64,2176]{1,0:T(8,128)(2,1)S(1)}, u32[]{:S(2)}, u32[]{:S(2)}) %collective-permute-start.8) | collective-permute-done | bytes 278560 | tf_op jit(solution)/shard_map/ppermute | solution.py:230
  18.2 0.7 %shard_map.96.refs_0_ = bf16[2,128,256]{2,1,0:T(8,128)(2,1)S(1)} custom-call(bf16[128,2176]{1,0:T(8,128)(2,1)S(1)} %shard_map.94.rows, bf16[64,2176]{1,0:T(8,128)(2,1)S(1)} %collective-permute-done.7.near, bf16[64,2176]{1,0:T(8,128)(2,1)S(1)} %collective-permute-done.8.far, f32[2,2,128,256]{3,2,1,0:T(8,128)S(1)} %shard_map.95.partial, ...), custom_call_target="tpu_custom_call" | custom-call | flops 536870912 | tf_op jit(solution)/shard_map/pallas_call | solution.py:178
  18.9 1.6 %collective-permute-start.9 = (bf16[2,128,256]{2,1,0:T(8,128)(2,1)S(1)}, bf16[2,128,256]{2,1,0:T(8,128)(2,1)S(1)}, u32[]{:S(2)}, u32[]{:S(2)}) collective-permute-start(bf16[2,128,256]{2,1,0:T(8,128)(2,1)S(1)} %shard_map.96.refs_0_), channel_id=1, source_target_pairs={{0,2},{1,3},{2,0},{3,1},{4,6},{5,7},{6,4},{7,5},{8,10},{9,11},{10,... | collective-permute-start | bytes 393224 | tf_op jit(solution)/shard_map/ppermute | solution.py:264
  20.5 0.0 collective-permute-start.11
  20.5 4.0 %collective-permute-done.9.refs_0_ = bf16[2,128,256]{2,1,0:T(8,128)(2,1)S(1)} collective-permute-done((bf16[2,128,256]{2,1,0:T(8,128)(2,1)S(1)}, bf16[2,128,256]{2,1,0:T(8,128)(2,1)S(1)}, u32[]{:S(2)}, u32[]{:S(2)}) %collective-permute-start.9) | collective-permute-done | bytes 131104 | tf_op jit(solution)/shard_map/ppermute | solution.py:264
  24.5 0.0 collective-permute-start.10
  24.5 0.0 collective-permute-done.11.refs_1_
  24.5 0.0 copy-done
  24.5 0.5 %shard_map.97.refs_3_ = f32[128,1024]{1,0:T(8,128)S(1)} custom-call(bf16[2,128,256]{2,1,0:T(8,128)(2,1)S(1)} %shard_map.96.refs_0_, bf16[2,128,256]{2,1,0:T(8,128)(2,1)S(1)} %collective-permute-done.11.refs_1_, bf16[2,1024,1024]{2,1,0:T(8,128)(2,1)S(1)} %copy-done), custom_call_target="tpu_custom_call" | custom-call | flops 100000000 | tf_op jit(solution)/shard_map/pallas_call | solution.py:178
  25.0 0.9 %collective-permute-done.10.refs_1_ = bf16[2,128,256]{2,1,0:T(8,128)(2,1)S(1)} collective-permute-done((bf16[2,128,256]{2,1,0:T(8,128)(2,1)S(1)}, bf16[2,128,256]{2,1,0:T(8,128)(2,1)S(1)}, u32[]{:S(2)}, u32[]{:S(2)}) %collective-permute-start.10) | collective-permute-done | bytes 131104 | tf_op jit(solution)/shard_map/ppermute | solution.py:230
  25.9 0.4 %shard_map.98 = (bf16[32,1024]{1,0:T(8,128)(2,1)S(1)}, bf16[32,1024]{1,0:T(8,128)(2,1)S(1)}, bf16[32,1024]{1,0:T(8,128)(2,1)S(1)}, bf16[32,1024]{1,0:T(8,128)(2,1)S(1)}) custom-call(bf16[2,128,256]{2,1,0:T(8,128)(2,1)S(1)} %collective-permute-done.9.refs_0_, bf16[2,128,256]{2,1,0:T(8,128)(2,1)S(1)} %collective-permute-done.10.refs_1_, ...), custom_call_target="tpu_custom_call" | custom-call | tf_op jit(solution)/shard_map/pallas_call | solution.py:178
  26.3 1.0 %collective-permute-start.12 = (bf16[32,1024]{1,0:T(8,128)(2,1)S(1)}, bf16[32,1024]{1,0:T(8,128)(2,1)S(1)}, u32[]{:S(2)}, u32[]{:S(2)}) collective-permute-start(bf16[32,1024]{1,0:T(8,128)(2,1)S(1)} %get-tuple-element.15), channel_id=1, source_target_pairs={{0,4},{4,0},{8,12},{12,8},{16,20},{20,16},{24,28},{28,24},{1,5},{5... | collective-permute-start | bytes 196616 | tf_op jit(solution)/shard_map/ppermute | solution.py:227
  27.4 1.0 %collective-permute-start.13 = (bf16[32,1024]{1,0:T(8,128)(2,1)S(1)}, bf16[32,1024]{1,0:T(8,128)(2,1)S(1)}, u32[]{:S(2)}, u32[]{:S(2)}) collective-permute-start(bf16[32,1024]{1,0:T(8,128)(2,1)S(1)} %get-tuple-element.16), channel_id=1, source_target_pairs={{0,8},{4,12},{8,0},{12,4},{16,24},{20,28},{24,16},{28,20},{1,9},{5... | collective-permute-start | bytes 196616 | tf_op jit(solution)/shard_map/ppermute | solution.py:227
  28.4 1.5 %collective-permute-start.14 = (bf16[32,1024]{1,0:T(8,128)(2,1)S(1)}, bf16[32,1024]{1,0:T(8,128)(2,1)S(1)}, u32[]{:S(2)}, u32[]{:S(2)}) collective-permute-start(bf16[32,1024]{1,0:T(8,128)(2,1)S(1)} %get-tuple-element.17), channel_id=1, source_target_pairs={{0,12},{4,8},{8,4},{12,0},{16,28},{20,24},{24,20},{28,16},{1,13},{... | collective-permute-start | bytes 196616 | tf_op jit(solution)/shard_map/ppermute | solution.py:227
  29.9 0.8 %collective-permute-done.12.refs_1_ = bf16[32,1024]{1,0:T(8,128)(2,1)S(1)} collective-permute-done((bf16[32,1024]{1,0:T(8,128)(2,1)S(1)}, bf16[32,1024]{1,0:T(8,128)(2,1)S(1)}, u32[]{:S(2)}, u32[]{:S(2)}) %collective-permute-start.12) | collective-permute-done | bytes 65568 | tf_op jit(solution)/shard_map/ppermute | solution.py:227
  30.6 1.1 %collective-permute-done.13.refs_2_ = bf16[32,1024]{1,0:T(8,128)(2,1)S(1)} collective-permute-done((bf16[32,1024]{1,0:T(8,128)(2,1)S(1)}, bf16[32,1024]{1,0:T(8,128)(2,1)S(1)}, u32[]{:S(2)}, u32[]{:S(2)}) %collective-permute-start.13) | collective-permute-done | bytes 65568 | tf_op jit(solution)/shard_map/ppermute | solution.py:227
  31.8 1.8 %collective-permute-done.14.refs_3_ = bf16[32,1024]{1,0:T(8,128)(2,1)S(1)} collective-permute-done((bf16[32,1024]{1,0:T(8,128)(2,1)S(1)}, bf16[32,1024]{1,0:T(8,128)(2,1)S(1)}, u32[]{:S(2)}, u32[]{:S(2)}) %collective-permute-start.14) | collective-permute-done | bytes 65568 | tf_op jit(solution)/shard_map/ppermute | solution.py:227
  33.6 2.9 %collective-permute-start.15 = (bf16[16,1024]{1,0:T(8,128)(2,1)S(1)}, bf16[16,1024]{1,0:T(8,128)(2,1)S(1)}, u32[]{:S(2)}, u32[]{:S(2)}) collective-permute-start(bf16[16,1024]{1,0:T(8,128)(2,1)S(1)} %shard_map.99), channel_id=1, source_target_pairs={{0,16},{4,20},{8,24},{12,28},{16,0},{20,4},{24,8},{28,12},{1,17},{... | collective-permute-start | bytes 98312 | tf_op jit(solution)/shard_map/ppermute | solution.py:224
  36.4 2.0 %collective-permute-done.15.refs_4_ = bf16[16,1024]{1,0:T(8,128)(2,1)S(1)} collective-permute-done((bf16[16,1024]{1,0:T(8,128)(2,1)S(1)}, bf16[16,1024]{1,0:T(8,128)(2,1)S(1)}, u32[]{:S(2)}, u32[]{:S(2)}) %collective-permute-start.15) | collective-permute-done | bytes 32800 | tf_op jit(solution)/shard_map/ppermute | solution.py:224
  38.5 0.8 %shard_map.100 = bf16[32,1024]{1,0:T(8,128)(2,1)} custom-call(bf16[32,1024]{1,0:T(8,128)(2,1)S(1)} %get-tuple-element.14.refs_0_, bf16[32,1024]{1,0:T(8,128)(2,1)S(1)} %collective-permute-done.12.refs_1_, bf16[32,1024]{1,0:T(8,128)(2,1)S(1)} %collective-permute-done.13.refs_2_, bf16[32,1024]{1,0:T(8,128)(2,1)S(1)} %collective-permute-done.14.refs_3_, ...), custom_call_target="tpu_custom_call" | custom-call | tf_op jit(solution)/shard_map/pallas_call | solution.py:178
  (4 shorter events, 0.1 us)
Async XLA Ops:
  0.0 16.7 %copy-start.1 = (bf16[2,4096,256]{2,1,0:T(8,128)(2,1)S(1)}, bf16[2,4096,256]{2,1,0:T(8,128)(2,1)}, u32[]{:S(2)}) copy-start(bf16[2,4096,256]{2,1,0:T(8,128)(2,1)} %w_gate.3) | copy-start | bytes 12582916
  0.0 16.7 %copy-start.2 = (bf16[2,4096,256]{2,1,0:T(8,128)(2,1)S(1)}, bf16[2,4096,256]{2,1,0:T(8,128)(2,1)}, u32[]{:S(2)}) copy-start(bf16[2,4096,256]{2,1,0:T(8,128)(2,1)} %w_up.3) | copy-start | bytes 12582916
  1.5 7.6 %collective-permute-start.3 = (bf16[16,2176]{1,0:T(8,128)(2,1)S(1)}, bf16[16,2176]{1,0:T(8,128)(2,1)S(1)}, u32[]{:S(2)}, u32[]{:S(2)}) collective-permute-start(bf16[16,2176]{1,0:T(8,128)(2,1)S(1)} %get-tuple-element.13), channel_id=1, source_target_pairs={{0,16},{4,20},{8,24},{12,28},{16,0},{20,4},{24,8},{28,12},{1,17},{... | collective-permute-start | bytes 208904 | tf_op jit(solution)/shard_map/ppermute | solution.py:224
  5.6 6.6 %collective-permute-start.2 = (bf16[16,2176]{1,0:T(8,128)(2,1)S(1)}, bf16[16,2176]{1,0:T(8,128)(2,1)S(1)}, u32[]{:S(2)}, u32[]{:S(2)}) collective-permute-start(bf16[16,2176]{1,0:T(8,128)(2,1)S(1)} %get-tuple-element.12.refs_0_), channel_id=1, source_target_pairs={{0,12},{4,8},{8,4},{12,0},{16,28},{20,24},{24,20},{28,16},{1,13},{... | collective-permute-start | bytes 208904 | tf_op jit(solution)/shard_map/ppermute | solution.py:227
  8.1 5.1 %collective-permute-start.1 = (bf16[16,2176]{1,0:T(8,128)(2,1)S(1)}, bf16[16,2176]{1,0:T(8,128)(2,1)S(1)}, u32[]{:S(2)}, u32[]{:S(2)}) collective-permute-start(bf16[16,2176]{1,0:T(8,128)(2,1)S(1)} %get-tuple-element.12.refs_0_), channel_id=1, source_target_pairs={{0,8},{4,12},{8,0},{12,4},{16,24},{20,28},{24,16},{28,20},{1,9},{5... | collective-permute-start | bytes 208904 | tf_op jit(solution)/shard_map/ppermute | solution.py:227
  8.6 5.3 %collective-permute-start = (bf16[16,2176]{1,0:T(8,128)(2,1)S(1)}, bf16[16,2176]{1,0:T(8,128)(2,1)S(1)}, u32[]{:S(2)}, u32[]{:S(2)}) collective-permute-start(bf16[16,2176]{1,0:T(8,128)(2,1)S(1)} %get-tuple-element.12.refs_0_), channel_id=1, source_target_pairs={{0,4},{4,0},{8,12},{12,8},{16,20},{20,16},{24,28},{28,24},{1,5},{5... | collective-permute-start | bytes 208904 | tf_op jit(solution)/shard_map/ppermute | solution.py:227
  9.1 5.6 %collective-permute-start.6 = (bf16[16,2176]{1,0:T(8,128)(2,1)S(1)}, bf16[16,2176]{1,0:T(8,128)(2,1)S(1)}, u32[]{:S(2)}, u32[]{:S(2)}) collective-permute-start(bf16[16,2176]{1,0:T(8,128)(2,1)S(1)} %collective-permute-done.3.refs_0_), channel_id=1, source_target_pairs={{0,12},{4,8},{8,4},{12,0},{16,28},{20,24},{24,20},{28,16},{1,13},{... | collective-permute-start | bytes 208904 | tf_op jit(solution)/shard_map/ppermute | solution.py:227
  11.6 4.3 %collective-permute-start.5 = (bf16[16,2176]{1,0:T(8,128)(2,1)S(1)}, bf16[16,2176]{1,0:T(8,128)(2,1)S(1)}, u32[]{:S(2)}, u32[]{:S(2)}) collective-permute-start(bf16[16,2176]{1,0:T(8,128)(2,1)S(1)} %collective-permute-done.3.refs_0_), channel_id=1, source_target_pairs={{0,8},{4,12},{8,0},{12,4},{16,24},{20,28},{24,16},{28,20},{1,9},{5... | collective-permute-start | bytes 208904 | tf_op jit(solution)/shard_map/ppermute | solution.py:227
  12.2 4.3 %collective-permute-start.4 = (bf16[16,2176]{1,0:T(8,128)(2,1)S(1)}, bf16[16,2176]{1,0:T(8,128)(2,1)S(1)}, u32[]{:S(2)}, u32[]{:S(2)}) collective-permute-start(bf16[16,2176]{1,0:T(8,128)(2,1)S(1)} %collective-permute-done.3.refs_0_), channel_id=1, source_target_pairs={{0,4},{4,0},{8,12},{12,8},{16,20},{20,16},{24,28},{28,24},{1,5},{5... | collective-permute-start | bytes 208904 | tf_op jit(solution)/shard_map/ppermute | solution.py:227
  13.9 3.5 %collective-permute-start.7 = (bf16[64,2176]{1,0:T(8,128)(2,1)S(1)}, bf16[64,2176]{1,0:T(8,128)(2,1)S(1)}, u32[]{:S(2)}, u32[]{:S(2)}) collective-permute-start(bf16[64,2176]{1,0:T(8,128)(2,1)S(1)} %shard_map.92.refs_0_), channel_id=1, source_target_pairs={{0,1},{1,0},{2,3},{3,2},{4,5},{5,4},{6,7},{7,6},{8,9},{9,8},{10,11... | collective-permute-start | bytes 835592 | tf_op jit(solution)/shard_map/ppermute | solution.py:230
  16.5 1.6 %collective-permute-start.8 = (bf16[64,2176]{1,0:T(8,128)(2,1)S(1)}, bf16[64,2176]{1,0:T(8,128)(2,1)S(1)}, u32[]{:S(2)}, u32[]{:S(2)}) collective-permute-start(bf16[64,2176]{1,0:T(8,128)(2,1)S(1)} %shard_map.93.refs_1_), channel_id=1, source_target_pairs={{0,1},{1,0},{2,3},{3,2},{4,5},{5,4},{6,7},{7,6},{8,9},{9,8},{10,11... | collective-permute-start | bytes 835592 | tf_op jit(solution)/shard_map/ppermute | solution.py:230
  17.4 7.1 %copy-start = (bf16[2,1024,1024]{2,1,0:T(8,128)(2,1)S(1)}, bf16[2,1024,1024]{2,1,0:T(8,128)(2,1)}, u32[]{:S(2)}) copy-start(bf16[2,1024,1024]{2,1,0:T(8,128)(2,1)} %refs_2_.3) | copy-start | bytes 12582916
  18.9 5.6 %collective-permute-start.9 = (bf16[2,128,256]{2,1,0:T(8,128)(2,1)S(1)}, bf16[2,128,256]{2,1,0:T(8,128)(2,1)S(1)}, u32[]{:S(2)}, u32[]{:S(2)}) collective-permute-start(bf16[2,128,256]{2,1,0:T(8,128)(2,1)S(1)} %shard_map.96.refs_0_), channel_id=1, source_target_pairs={{0,2},{1,3},{2,0},{3,1},{4,6},{5,7},{6,4},{7,5},{8,10},{9,11},{10,... | collective-permute-start | bytes 393224 | tf_op jit(solution)/shard_map/ppermute | solution.py:264
  20.5 4.0 %collective-permute-start.11 = (bf16[2,128,256]{2,1,0:T(8,128)(2,1)S(1)}, bf16[2,128,256]{2,1,0:T(8,128)(2,1)S(1)}, u32[]{:S(2)}, u32[]{:S(2)}) collective-permute-start(bf16[2,128,256]{2,1,0:T(8,128)(2,1)S(1)} %shard_map.96.refs_0_), channel_id=1, source_target_pairs={{0,1},{1,0},{2,3},{3,2},{4,5},{5,4},{6,7},{7,6},{8,9},{9,8},{10,11... | collective-permute-start | bytes 393224 | tf_op jit(solution)/shard_map/ppermute | solution.py:230
  24.5 1.3 %collective-permute-start.10 = (bf16[2,128,256]{2,1,0:T(8,128)(2,1)S(1)}, bf16[2,128,256]{2,1,0:T(8,128)(2,1)S(1)}, u32[]{:S(2)}, u32[]{:S(2)}) collective-permute-start(bf16[2,128,256]{2,1,0:T(8,128)(2,1)S(1)} %collective-permute-done.9.refs_0_), channel_id=1, source_target_pairs={{0,1},{1,0},{2,3},{3,2},{4,5},{5,4},{6,7},{7,6},{8,9},{9,8},{10,11... | collective-permute-start | bytes 393224 | tf_op jit(solution)/shard_map/ppermute | solution.py:230
  26.3 4.3 %collective-permute-start.12 = (bf16[32,1024]{1,0:T(8,128)(2,1)S(1)}, bf16[32,1024]{1,0:T(8,128)(2,1)S(1)}, u32[]{:S(2)}, u32[]{:S(2)}) collective-permute-start(bf16[32,1024]{1,0:T(8,128)(2,1)S(1)} %get-tuple-element.15), channel_id=1, source_target_pairs={{0,4},{4,0},{8,12},{12,8},{16,20},{20,16},{24,28},{28,24},{1,5},{5... | collective-permute-start | bytes 196616 | tf_op jit(solution)/shard_map/ppermute | solution.py:227
  27.4 4.4 %collective-permute-start.13 = (bf16[32,1024]{1,0:T(8,128)(2,1)S(1)}, bf16[32,1024]{1,0:T(8,128)(2,1)S(1)}, u32[]{:S(2)}, u32[]{:S(2)}) collective-permute-start(bf16[32,1024]{1,0:T(8,128)(2,1)S(1)} %get-tuple-element.16), channel_id=1, source_target_pairs={{0,8},{4,12},{8,0},{12,4},{16,24},{20,28},{24,16},{28,20},{1,9},{5... | collective-permute-start | bytes 196616 | tf_op jit(solution)/shard_map/ppermute | solution.py:227
  28.4 5.2 %collective-permute-start.14 = (bf16[32,1024]{1,0:T(8,128)(2,1)S(1)}, bf16[32,1024]{1,0:T(8,128)(2,1)S(1)}, u32[]{:S(2)}, u32[]{:S(2)}) collective-permute-start(bf16[32,1024]{1,0:T(8,128)(2,1)S(1)} %get-tuple-element.17), channel_id=1, source_target_pairs={{0,12},{4,8},{8,4},{12,0},{16,28},{20,24},{24,20},{28,16},{1,13},{... | collective-permute-start | bytes 196616 | tf_op jit(solution)/shard_map/ppermute | solution.py:227
  33.6 4.9 %collective-permute-start.15 = (bf16[16,1024]{1,0:T(8,128)(2,1)S(1)}, bf16[16,1024]{1,0:T(8,128)(2,1)S(1)}, u32[]{:S(2)}, u32[]{:S(2)}) collective-permute-start(bf16[16,1024]{1,0:T(8,128)(2,1)S(1)} %shard_map.99), channel_id=1, source_target_pairs={{0,16},{4,20},{8,24},{12,28},{16,0},{20,4},{24,8},{28,12},{1,17},{... | collective-permute-start | bytes 98312 | tf_op jit(solution)/shard_map/ppermute | solution.py:224

commit v2 on v1

--- a/solution.py
+++ b/solution.py
@@ -146,9 +146,9 @@
     return total
 
 
-def down_kernel(*refs, steps):
-    acts, w_down, out = refs[: len(steps)], refs[-2], refs[-1]
-    out[...] = down_sum(acts, w_down, steps)
+def down_kernel(*refs, steps, base=False):
+    acts, w_down, out = refs[: len(steps)], refs[len(steps)], refs[-1]
+    out[...] = down_sum(acts, w_down, steps, refs[-2][...] if base else None)
 
 
 def down_last_kernel(*refs, steps, owners, capacity):
@@ -274,12 +274,20 @@
         (act, near, w_down),
         flops=10**8,
     )
+    direct = tuple(step for step in steps[2:] if not step[1])
+    swapped = tuple(step for step in steps[2:] if step[1])
+    base = kernel_call(
+        functools.partial(down_kernel, steps=direct, base=True),
+        shape((count, out_cols), F32),
+        (*far[::2], w_down, base),
+        flops=10**8,
+    )
     sums = kernel_call(
         functools.partial(
-            down_last_kernel, steps=steps[2:], owners=owners, capacity=capacity
+            down_last_kernel, steps=swapped, owners=owners, capacity=capacity
         ),
         [shape((count // owners, out_cols), BF16)] * owners,
-        (*far, w_down, base),
+        (*far[1::2], w_down, base),
     )
     gathered = [sums[0]]
     for j in reversed(range(1, owners)):

time: 39.4 us -> 39.3 us (level)
    pallas_call x10 -> x11, Pallas kernels: 4.79 us -> 4.98 us  [kernel_call(): pl.pallas_call(body, out_shape=out_shape, in_specs=[pl.BlockSpec(memory_s...]
  transfers between devices with their start and end apart: 16 -> 16, of which waited for: 11 -> 11; matrix products, arithmetic and copies ran while one was open for 0% -> 0% of each run, Pallas kernels for 3% -> 4%
where the time goes in v2:
time: 39.3 us; the launch traced here: 39.2 us
  starting transfers between devices  19.8 us (50%)
  waiting for transfers between devices  14.2 us (36%)
  Pallas kernels  4.98 us (13%)
    ppermute x9, starting transfers between devices, to_owner(): return lax.ppermute(value, 'ep', [(s, s ^ j) for s in range(ep_count)])  11.1 us
    ppermute x2, starting transfers between devices, shift_group(): return lax.ppermute(value, 'ep', pairs)  7 us
    ppermute x9, waiting for transfers between devices, to_owner(): return lax.ppermute(value, 'ep', [(s, s ^ j) for s in range(ep_count)])  6.9 us
    pallas_call x11, Pallas kernels, kernel_call(): pl.pallas_call(body, out_shape=out_shape, in_specs=[pl.BlockSpec(memory_s...  4.98 us
    ppermute x1, waiting for transfers between devices, on_device(): lax.ppermute(act, 'tp', [(t, (t + 2 * d) % tp_count) for t in range(tp_co...  4.02 us
    ppermute x2, waiting for transfers between devices, shift_group(): return lax.ppermute(value, 'ep', pairs)  2.01 us
    ppermute x1, starting transfers between devices, on_device(): lax.ppermute(act, 'tp', [(t, (t + 2 * d) % tp_count) for t in range(tp_co...  1.58 us
    ppermute x4, waiting for transfers between devices, swap_cores(): return lax.ppermute(value, 'tp', [(t, t ^ 1) for t in range(tp_count)])  1.28 us
  transfers between devices with their start and end apart: 16, of which 11 were waited for; matrix products, arithmetic and copies ran while one was open for 0% of the time, Pallas kernels for 4%

profile of v2, /device:TPU:0, one launch (start us, length us, event | category | flops | bytes accessed | tf_op | source)
XLA Modules:
  0.0 39.2 jit_solution(8816616171284240390)
XLA Ops:
  0.0 0.0 copy-start.1
  0.0 0.0 copy-start.2
  0.0 1.5 %shard_map.91 = (bf16[16,2176]{1,0:T(8,128)(2,1)S(1)}, bf16[16,2176]{1,0:T(8,128)(2,1)S(1)}, bf16[32,32]{1,0:T(8,128)(2,1)S(1)}) custom-call(bf16[32,4096]{1,0:T(8,128)(2,1)} %refs_0_.1, f32[1,4096]{1,0:T(1,128)} %bitcast.5, s32[1,32]{1,0:T(1,128)} %bitcast.8, s32[4,32]{1,0:T(4,128)} %bitcast.6, f32[1,32]{1,0:T(1,128)} %bitcast.9, f32[4,32]{1,0:T(4,128)} %bitcast.7), custom_call_target="tpu_custom_call" | custom-call | flops 10000000000 | tf_op jit(solution)/shard_map/pallas_call | solution.py:178
  1.5 4.1 %collective-permute-start.3 = (bf16[16,2176]{1,0:T(8,128)(2,1)S(1)}, bf16[16,2176]{1,0:T(8,128)(2,1)S(1)}, u32[]{:S(2)}, u32[]{:S(2)}) collective-permute-start(bf16[16,2176]{1,0:T(8,128)(2,1)S(1)} %get-tuple-element.13), channel_id=1, source_target_pairs={{0,16},{4,20},{8,24},{12,28},{16,0},{20,4},{24,8},{28,12},{1,17},{... | collective-permute-start | bytes 208904 | tf_op jit(solution)/shard_map/ppermute | solution.py:224
  5.6 2.5 %collective-permute-start.2 = (bf16[16,2176]{1,0:T(8,128)(2,1)S(1)}, bf16[16,2176]{1,0:T(8,128)(2,1)S(1)}, u32[]{:S(2)}, u32[]{:S(2)}) collective-permute-start(bf16[16,2176]{1,0:T(8,128)(2,1)S(1)} %get-tuple-element.12.refs_0_), channel_id=1, source_target_pairs={{0,12},{4,8},{8,4},{12,0},{16,28},{20,24},{24,20},{28,16},{1,13},{... | collective-permute-start | bytes 208904 | tf_op jit(solution)/shard_map/ppermute | solution.py:227
  8.1 0.4 %collective-permute-start.1 = (bf16[16,2176]{1,0:T(8,128)(2,1)S(1)}, bf16[16,2176]{1,0:T(8,128)(2,1)S(1)}, u32[]{:S(2)}, u32[]{:S(2)}) collective-permute-start(bf16[16,2176]{1,0:T(8,128)(2,1)S(1)} %get-tuple-element.12.refs_0_), channel_id=1, source_target_pairs={{0,8},{4,12},{8,0},{12,4},{16,24},{20,28},{24,16},{28,20},{1,9},{5... | collective-permute-start | bytes 208904 | tf_op jit(solution)/shard_map/ppermute | solution.py:227
  8.6 0.5 %collective-permute-start = (bf16[16,2176]{1,0:T(8,128)(2,1)S(1)}, bf16[16,2176]{1,0:T(8,128)(2,1)S(1)}, u32[]{:S(2)}, u32[]{:S(2)}) collective-permute-start(bf16[16,2176]{1,0:T(8,128)(2,1)S(1)} %get-tuple-element.12.refs_0_), channel_id=1, source_target_pairs={{0,4},{4,0},{8,12},{12,8},{16,20},{20,16},{24,28},{28,24},{1,5},{5... | collective-permute-start | bytes 208904 | tf_op jit(solution)/shard_map/ppermute | solution.py:227
  9.1 0.0 collective-permute-done.3.refs_0_
  9.1 2.5 %collective-permute-start.6 = (bf16[16,2176]{1,0:T(8,128)(2,1)S(1)}, bf16[16,2176]{1,0:T(8,128)(2,1)S(1)}, u32[]{:S(2)}, u32[]{:S(2)}) collective-permute-start(bf16[16,2176]{1,0:T(8,128)(2,1)S(1)} %collective-permute-done.3.refs_0_), channel_id=1, source_target_pairs={{0,12},{4,8},{8,4},{12,0},{16,28},{20,24},{24,20},{28,16},{1,13},{... | collective-permute-start | bytes 208904 | tf_op jit(solution)/shard_map/ppermute | solution.py:227
  11.6 0.6 %collective-permute-start.5 = (bf16[16,2176]{1,0:T(8,128)(2,1)S(1)}, bf16[16,2176]{1,0:T(8,128)(2,1)S(1)}, u32[]{:S(2)}, u32[]{:S(2)}) collective-permute-start(bf16[16,2176]{1,0:T(8,128)(2,1)S(1)} %collective-permute-done.3.refs_0_), channel_id=1, source_target_pairs={{0,8},{4,12},{8,0},{12,4},{16,24},{20,28},{24,16},{28,20},{1,9},{5... | collective-permute-start | bytes 208904 | tf_op jit(solution)/shard_map/ppermute | solution.py:227
  12.2 0.0 collective-permute-done.2.refs_3_
  12.2 1.0 %collective-permute-start.4 = (bf16[16,2176]{1,0:T(8,128)(2,1)S(1)}, bf16[16,2176]{1,0:T(8,128)(2,1)S(1)}, u32[]{:S(2)}, u32[]{:S(2)}) collective-permute-start(bf16[16,2176]{1,0:T(8,128)(2,1)S(1)} %collective-permute-done.3.refs_0_), channel_id=1, source_target_pairs={{0,4},{4,0},{8,12},{12,8},{16,20},{20,16},{24,28},{28,24},{1,5},{5... | collective-permute-start | bytes 208904 | tf_op jit(solution)/shard_map/ppermute | solution.py:227
  13.2 0.0 collective-permute-done.1.refs_2_
  13.2 0.7 %collective-permute-done.refs_1_ = bf16[16,2176]{1,0:T(8,128)(2,1)S(1)} collective-permute-done((bf16[16,2176]{1,0:T(8,128)(2,1)S(1)}, bf16[16,2176]{1,0:T(8,128)(2,1)S(1)}, u32[]{:S(2)}, u32[]{:S(2)}) %collective-permute-start) | collective-permute-done | bytes 69664 | tf_op jit(solution)/shard_map/ppermute | solution.py:227
  13.9 0.1 collective-permute-start.7
  14.0 0.7 %collective-permute-done.6.refs_3_ = bf16[16,2176]{1,0:T(8,128)(2,1)S(1)} collective-permute-done((bf16[16,2176]{1,0:T(8,128)(2,1)S(1)}, bf16[16,2176]{1,0:T(8,128)(2,1)S(1)}, u32[]{:S(2)}, u32[]{:S(2)}) %collective-permute-start.6) | collective-permute-done | bytes 69664 | tf_op jit(solution)/shard_map/ppermute | solution.py:227
  14.7 1.2 %collective-permute-done.5.refs_2_ = bf16[16,2176]{1,0:T(8,128)(2,1)S(1)} collective-permute-done((bf16[16,2176]{1,0:T(8,128)(2,1)S(1)}, bf16[16,2176]{1,0:T(8,128)(2,1)S(1)}, u32[]{:S(2)}, u32[]{:S(2)}) %collective-permute-start.5) | collective-permute-done | bytes 69664 | tf_op jit(solution)/shard_map/ppermute | solution.py:227
  15.9 0.6 %collective-permute-done.4.refs_1_ = bf16[16,2176]{1,0:T(8,128)(2,1)S(1)} collective-permute-done((bf16[16,2176]{1,0:T(8,128)(2,1)S(1)}, bf16[16,2176]{1,0:T(8,128)(2,1)S(1)}, u32[]{:S(2)}, u32[]{:S(2)}) %collective-permute-start.4) | collective-permute-done | bytes 69664 | tf_op jit(solution)/shard_map/ppermute | solution.py:227
  16.5 0.1 collective-permute-start.8
  16.7 0.0 copy-done.1
  16.7 0.0 copy-done.2
  16.7 0.7 %shard_map.95.partial = f32[2,2,128,256]{3,2,1,0:T(8,128)S(1)} custom-call(bf16[128,2176]{1,0:T(8,128)(2,1)S(1)} %shard_map.94.rows, bf16[2,4096,256]{2,1,0:T(8,128)(2,1)S(1)} %copy-done.1, bf16[2,4096,256]{2,1,0:T(8,128)(2,1)S(1)} %copy-done.2), custom_call_target="tpu_custom_call" | custom-call | flops 536870912 | tf_op jit(solution)/shard_map/pallas_call | solution.py:178
  17.4 0.0 copy-start
  17.4 0.0 collective-permute-done.7.near
  17.4 0.7 %collective-permute-done.8.far = bf16[64,2176]{1,0:T(8,128)(2,1)S(1)} collective-permute-done((bf16[64,2176]{1,0:T(8,128)(2,1)S(1)}, bf16[64,2176]{1,0:T(8,128)(2,1)S(1)}, u32[]{:S(2)}, u32[]{:S(2)}) %collective-permute-start.8) | collective-permute-done | bytes 278560 | tf_op jit(solution)/shard_map/ppermute | solution.py:230
  18.2 0.7 %shard_map.96.refs_0_ = bf16[2,128,256]{2,1,0:T(8,128)(2,1)S(1)} custom-call(bf16[128,2176]{1,0:T(8,128)(2,1)S(1)} %shard_map.94.rows, bf16[64,2176]{1,0:T(8,128)(2,1)S(1)} %collective-permute-done.7.near, bf16[64,2176]{1,0:T(8,128)(2,1)S(1)} %collective-permute-done.8.far, f32[2,2,128,256]{3,2,1,0:T(8,128)S(1)} %shard_map.95.partial, ...), custom_call_target="tpu_custom_call" | custom-call | flops 536870912 | tf_op jit(solution)/shard_map/pallas_call | solution.py:178
  18.9 1.6 %collective-permute-start.9 = (bf16[2,128,256]{2,1,0:T(8,128)(2,1)S(1)}, bf16[2,128,256]{2,1,0:T(8,128)(2,1)S(1)}, u32[]{:S(2)}, u32[]{:S(2)}) collective-permute-start(bf16[2,128,256]{2,1,0:T(8,128)(2,1)S(1)} %shard_map.96.refs_0_), channel_id=1, source_target_pairs={{0,2},{1,3},{2,0},{3,1},{4,6},{5,7},{6,4},{7,5},{8,10},{9,11},{10,... | collective-permute-start | bytes 393224 | tf_op jit(solution)/shard_map/ppermute | solution.py:264
  20.5 0.0 collective-permute-start.11
  20.5 4.0 %collective-permute-done.9.refs_0_ = bf16[2,128,256]{2,1,0:T(8,128)(2,1)S(1)} collective-permute-done((bf16[2,128,256]{2,1,0:T(8,128)(2,1)S(1)}, bf16[2,128,256]{2,1,0:T(8,128)(2,1)S(1)}, u32[]{:S(2)}, u32[]{:S(2)}) %collective-permute-start.9) | collective-permute-done | bytes 131104 | tf_op jit(solution)/shard_map/ppermute | solution.py:264
  24.5 0.0 collective-permute-start.10
  24.5 0.0 collective-permute-done.11.refs_1_
  24.5 0.0 copy-done
  24.5 0.5 %shard_map.97.refs_2_ = f32[128,1024]{1,0:T(8,128)S(1)} custom-call(bf16[2,128,256]{2,1,0:T(8,128)(2,1)S(1)} %shard_map.96.refs_0_, bf16[2,128,256]{2,1,0:T(8,128)(2,1)S(1)} %collective-permute-done.11.refs_1_, bf16[2,1024,1024]{2,1,0:T(8,128)(2,1)S(1)} %copy-done), custom_call_target="tpu_custom_call" | custom-call | flops 100000000 | tf_op jit(solution)/shard_map/pallas_call | solution.py:178
  25.0 0.3 shard_map.98.refs_2_
  25.3 0.5 %collective-permute-done.10.refs_0_ = bf16[2,128,256]{2,1,0:T(8,128)(2,1)S(1)} collective-permute-done((bf16[2,128,256]{2,1,0:T(8,128)(2,1)S(1)}, bf16[2,128,256]{2,1,0:T(8,128)(2,1)S(1)}, u32[]{:S(2)}, u32[]{:S(2)}) %collective-permute-start.10) | collective-permute-done | bytes 131104 | tf_op jit(solution)/shard_map/ppermute | solution.py:230
  25.9 0.3 shard_map.99
  26.2 1.0 %collective-permute-start.12 = (bf16[32,1024]{1,0:T(8,128)(2,1)S(1)}, bf16[32,1024]{1,0:T(8,128)(2,1)S(1)}, u32[]{:S(2)}, u32[]{:S(2)}) collective-permute-start(bf16[32,1024]{1,0:T(8,128)(2,1)S(1)} %get-tuple-element.15), channel_id=1, source_target_pairs={{0,4},{4,0},{8,12},{12,8},{16,20},{20,16},{24,28},{28,24},{1,5},{5... | collective-permute-start | bytes 196616 | tf_op jit(solution)/shard_map/ppermute | solution.py:227
  27.2 1.0 %collective-permute-start.13 = (bf16[32,1024]{1,0:T(8,128)(2,1)S(1)}, bf16[32,1024]{1,0:T(8,128)(2,1)S(1)}, u32[]{:S(2)}, u32[]{:S(2)}) collective-permute-start(bf16[32,1024]{1,0:T(8,128)(2,1)S(1)} %get-tuple-element.16), channel_id=1, source_target_pairs={{0,8},{4,12},{8,0},{12,4},{16,24},{20,28},{24,16},{28,20},{1,9},{5... | collective-permute-start | bytes 196616 | tf_op jit(solution)/shard_map/ppermute | solution.py:227
  28.2 1.5 %collective-permute-start.14 = (bf16[32,1024]{1,0:T(8,128)(2,1)S(1)}, bf16[32,1024]{1,0:T(8,128)(2,1)S(1)}, u32[]{:S(2)}, u32[]{:S(2)}) collective-permute-start(bf16[32,1024]{1,0:T(8,128)(2,1)S(1)} %get-tuple-element.17), channel_id=1, source_target_pairs={{0,12},{4,8},{8,4},{12,0},{16,28},{20,24},{24,20},{28,16},{1,13},{... | collective-permute-start | bytes 196616 | tf_op jit(solution)/shard_map/ppermute | solution.py:227
  29.7 0.8 %collective-permute-done.12.refs_1_ = bf16[32,1024]{1,0:T(8,128)(2,1)S(1)} collective-permute-done((bf16[32,1024]{1,0:T(8,128)(2,1)S(1)}, bf16[32,1024]{1,0:T(8,128)(2,1)S(1)}, u32[]{:S(2)}, u32[]{:S(2)}) %collective-permute-start.12) | collective-permute-done | bytes 65568 | tf_op jit(solution)/shard_map/ppermute | solution.py:227
  30.5 1.1 %collective-permute-done.13.refs_2_ = bf16[32,1024]{1,0:T(8,128)(2,1)S(1)} collective-permute-done((bf16[32,1024]{1,0:T(8,128)(2,1)S(1)}, bf16[32,1024]{1,0:T(8,128)(2,1)S(1)}, u32[]{:S(2)}, u32[]{:S(2)}) %collective-permute-start.13) | collective-permute-done | bytes 65568 | tf_op jit(solution)/shard_map/ppermute | solution.py:227
  31.6 1.8 %collective-permute-done.14.refs_3_ = bf16[32,1024]{1,0:T(8,128)(2,1)S(1)} collective-permute-done((bf16[32,1024]{1,0:T(8,128)(2,1)S(1)}, bf16[32,1024]{1,0:T(8,128)(2,1)S(1)}, u32[]{:S(2)}, u32[]{:S(2)}) %collective-permute-start.14) | collective-permute-done | bytes 65568 | tf_op jit(solution)/shard_map/ppermute | solution.py:227
  33.4 2.9 %collective-permute-start.15 = (bf16[16,1024]{1,0:T(8,128)(2,1)S(1)}, bf16[16,1024]{1,0:T(8,128)(2,1)S(1)}, u32[]{:S(2)}, u32[]{:S(2)}) collective-permute-start(bf16[16,1024]{1,0:T(8,128)(2,1)S(1)} %shard_map.100), channel_id=1, source_target_pairs={{0,16},{4,20},{8,24},{12,28},{16,0},{20,4},{24,8},{28,12},{1,17},{... | collective-permute-start | bytes 98312 | tf_op jit(solution)/shard_map/ppermute | solution.py:224
  36.3 2.0 %collective-permute-done.15.refs_4_ = bf16[16,1024]{1,0:T(8,128)(2,1)S(1)} collective-permute-done((bf16[16,1024]{1,0:T(8,128)(2,1)S(1)}, bf16[16,1024]{1,0:T(8,128)(2,1)S(1)}, u32[]{:S(2)}, u32[]{:S(2)}) %collective-permute-start.15) | collective-permute-done | bytes 32800 | tf_op jit(solution)/shard_map/ppermute | solution.py:224
  38.3 0.8 %shard_map.101 = bf16[32,1024]{1,0:T(8,128)(2,1)} custom-call(bf16[32,1024]{1,0:T(8,128)(2,1)S(1)} %get-tuple-element.14.refs_0_, bf16[32,1024]{1,0:T(8,128)(2,1)S(1)} %collective-permute-done.12.refs_1_, bf16[32,1024]{1,0:T(8,128)(2,1)S(1)} %collective-permute-done.13.refs_2_, bf16[32,1024]{1,0:T(8,128)(2,1)S(1)} %collective-permute-done.14.refs_3_, ...), custom_call_target="tpu_custom_call" | custom-call | tf_op jit(solution)/shard_map/pallas_call | solution.py:178
  (4 shorter events, 0.1 us)
Async XLA Ops:
  0.0 16.7 %copy-start.1 = (bf16[2,4096,256]{2,1,0:T(8,128)(2,1)S(1)}, bf16[2,4096,256]{2,1,0:T(8,128)(2,1)}, u32[]{:S(2)}) copy-start(bf16[2,4096,256]{2,1,0:T(8,128)(2,1)} %w_gate.3) | copy-start | bytes 12582916
  0.0 16.7 %copy-start.2 = (bf16[2,4096,256]{2,1,0:T(8,128)(2,1)S(1)}, bf16[2,4096,256]{2,1,0:T(8,128)(2,1)}, u32[]{:S(2)}) copy-start(bf16[2,4096,256]{2,1,0:T(8,128)(2,1)} %w_up.3) | copy-start | bytes 12582916
  1.5 7.6 %collective-permute-start.3 = (bf16[16,2176]{1,0:T(8,128)(2,1)S(1)}, bf16[16,2176]{1,0:T(8,128)(2,1)S(1)}, u32[]{:S(2)}, u32[]{:S(2)}) collective-permute-start(bf16[16,2176]{1,0:T(8,128)(2,1)S(1)} %get-tuple-element.13), channel_id=1, source_target_pairs={{0,16},{4,20},{8,24},{12,28},{16,0},{20,4},{24,8},{28,12},{1,17},{... | collective-permute-start | bytes 208904 | tf_op jit(solution)/shard_map/ppermute | solution.py:224
  5.6 6.6 %collective-permute-start.2 = (bf16[16,2176]{1,0:T(8,128)(2,1)S(1)}, bf16[16,2176]{1,0:T(8,128)(2,1)S(1)}, u32[]{:S(2)}, u32[]{:S(2)}) collective-permute-start(bf16[16,2176]{1,0:T(8,128)(2,1)S(1)} %get-tuple-element.12.refs_0_), channel_id=1, source_target_pairs={{0,12},{4,8},{8,4},{12,0},{16,28},{20,24},{24,20},{28,16},{1,13},{... | collective-permute-start | bytes 208904 | tf_op jit(solution)/shard_map/ppermute | solution.py:227
  8.1 5.1 %collective-permute-start.1 = (bf16[16,2176]{1,0:T(8,128)(2,1)S(1)}, bf16[16,2176]{1,0:T(8,128)(2,1)S(1)}, u32[]{:S(2)}, u32[]{:S(2)}) collective-permute-start(bf16[16,2176]{1,0:T(8,128)(2,1)S(1)} %get-tuple-element.12.refs_0_), channel_id=1, source_target_pairs={{0,8},{4,12},{8,0},{12,4},{16,24},{20,28},{24,16},{28,20},{1,9},{5... | collective-permute-start | bytes 208904 | tf_op jit(solution)/shard_map/ppermute | solution.py:227
  8.6 5.3 %collective-permute-start = (bf16[16,2176]{1,0:T(8,128)(2,1)S(1)}, bf16[16,2176]{1,0:T(8,128)(2,1)S(1)}, u32[]{:S(2)}, u32[]{:S(2)}) collective-permute-start(bf16[16,2176]{1,0:T(8,128)(2,1)S(1)} %get-tuple-element.12.refs_0_), channel_id=1, source_target_pairs={{0,4},{4,0},{8,12},{12,8},{16,20},{20,16},{24,28},{28,24},{1,5},{5... | collective-permute-start | bytes 208904 | tf_op jit(solution)/shard_map/ppermute | solution.py:227
  9.1 5.6 %collective-permute-start.6 = (bf16[16,2176]{1,0:T(8,128)(2,1)S(1)}, bf16[16,2176]{1,0:T(8,128)(2,1)S(1)}, u32[]{:S(2)}, u32[]{:S(2)}) collective-permute-start(bf16[16,2176]{1,0:T(8,128)(2,1)S(1)} %collective-permute-done.3.refs_0_), channel_id=1, source_target_pairs={{0,12},{4,8},{8,4},{12,0},{16,28},{20,24},{24,20},{28,16},{1,13},{... | collective-permute-start | bytes 208904 | tf_op jit(solution)/shard_map/ppermute | solution.py:227
  11.6 4.3 %collective-permute-start.5 = (bf16[16,2176]{1,0:T(8,128)(2,1)S(1)}, bf16[16,2176]{1,0:T(8,128)(2,1)S(1)}, u32[]{:S(2)}, u32[]{:S(2)}) collective-permute-start(bf16[16,2176]{1,0:T(8,128)(2,1)S(1)} %collective-permute-done.3.refs_0_), channel_id=1, source_target_pairs={{0,8},{4,12},{8,0},{12,4},{16,24},{20,28},{24,16},{28,20},{1,9},{5... | collective-permute-start | bytes 208904 | tf_op jit(solution)/shard_map/ppermute | solution.py:227
  12.2 4.3 %collective-permute-start.4 = (bf16[16,2176]{1,0:T(8,128)(2,1)S(1)}, bf16[16,2176]{1,0:T(8,128)(2,1)S(1)}, u32[]{:S(2)}, u32[]{:S(2)}) collective-permute-start(bf16[16,2176]{1,0:T(8,128)(2,1)S(1)} %collective-permute-done.3.refs_0_), channel_id=1, source_target_pairs={{0,4},{4,0},{8,12},{12,8},{16,20},{20,16},{24,28},{28,24},{1,5},{5... | collective-permute-start | bytes 208904 | tf_op jit(solution)/shard_map/ppermute | solution.py:227
  13.9 3.5 %collective-permute-start.7 = (bf16[64,2176]{1,0:T(8,128)(2,1)S(1)}, bf16[64,2176]{1,0:T(8,128)(2,1)S(1)}, u32[]{:S(2)}, u32[]{:S(2)}) collective-permute-start(bf16[64,2176]{1,0:T(8,128)(2,1)S(1)} %shard_map.92.refs_0_), channel_id=1, source_target_pairs={{0,1},{1,0},{2,3},{3,2},{4,5},{5,4},{6,7},{7,6},{8,9},{9,8},{10,11... | collective-permute-start | bytes 835592 | tf_op jit(solution)/shard_map/ppermute | solution.py:230
  16.5 1.6 %collective-permute-start.8 = (bf16[64,2176]{1,0:T(8,128)(2,1)S(1)}, bf16[64,2176]{1,0:T(8,128)(2,1)S(1)}, u32[]{:S(2)}, u32[]{:S(2)}) collective-permute-start(bf16[64,2176]{1,0:T(8,128)(2,1)S(1)} %shard_map.93.refs_1_), channel_id=1, source_target_pairs={{0,1},{1,0},{2,3},{3,2},{4,5},{5,4},{6,7},{7,6},{8,9},{9,8},{10,11... | collective-permute-start | bytes 835592 | tf_op jit(solution)/shard_map/ppermute | solution.py:230
  17.4 7.1 %copy-start = (bf16[2,1024,1024]{2,1,0:T(8,128)(2,1)S(1)}, bf16[2,1024,1024]{2,1,0:T(8,128)(2,1)}, u32[]{:S(2)}) copy-start(bf16[2,1024,1024]{2,1,0:T(8,128)(2,1)} %refs_1_.3) | copy-start | bytes 12582916
  18.9 5.6 %collective-permute-start.9 = (bf16[2,128,256]{2,1,0:T(8,128)(2,1)S(1)}, bf16[2,128,256]{2,1,0:T(8,128)(2,1)S(1)}, u32[]{:S(2)}, u32[]{:S(2)}) collective-permute-start(bf16[2,128,256]{2,1,0:T(8,128)(2,1)S(1)} %shard_map.96.refs_0_), channel_id=1, source_target_pairs={{0,2},{1,3},{2,0},{3,1},{4,6},{5,7},{6,4},{7,5},{8,10},{9,11},{10,... | collective-permute-start | bytes 393224 | tf_op jit(solution)/shard_map/ppermute | solution.py:264
  20.5 4.0 %collective-permute-start.11 = (bf16[2,128,256]{2,1,0:T(8,128)(2,1)S(1)}, bf16[2,128,256]{2,1,0:T(8,128)(2,1)S(1)}, u32[]{:S(2)}, u32[]{:S(2)}) collective-permute-start(bf16[2,128,256]{2,1,0:T(8,128)(2,1)S(1)} %shard_map.96.refs_0_), channel_id=1, source_target_pairs={{0,1},{1,0},{2,3},{3,2},{4,5},{5,4},{6,7},{7,6},{8,9},{9,8},{10,11... | collective-permute-start | bytes 393224 | tf_op jit(solution)/shard_map/ppermute | solution.py:230
  24.5 1.3 %collective-permute-start.10 = (bf16[2,128,256]{2,1,0:T(8,128)(2,1)S(1)}, bf16[2,128,256]{2,1,0:T(8,128)(2,1)S(1)}, u32[]{:S(2)}, u32[]{:S(2)}) collective-permute-start(bf16[2,128,256]{2,1,0:T(8,128)(2,1)S(1)} %collective-permute-done.9.refs_0_), channel_id=1, source_target_pairs={{0,1},{1,0},{2,3},{3,2},{4,5},{5,4},{6,7},{7,6},{8,9},{9,8},{10,11... | collective-permute-start | bytes 393224 | tf_op jit(solution)/shard_map/ppermute | solution.py:230
  26.2 4.3 %collective-permute-start.12 = (bf16[32,1024]{1,0:T(8,128)(2,1)S(1)}, bf16[32,1024]{1,0:T(8,128)(2,1)S(1)}, u32[]{:S(2)}, u32[]{:S(2)}) collective-permute-start(bf16[32,1024]{1,0:T(8,128)(2,1)S(1)} %get-tuple-element.15), channel_id=1, source_target_pairs={{0,4},{4,0},{8,12},{12,8},{16,20},{20,16},{24,28},{28,24},{1,5},{5... | collective-permute-start | bytes 196616 | tf_op jit(solution)/shard_map/ppermute | solution.py:227
  27.2 4.4 %collective-permute-start.13 = (bf16[32,1024]{1,0:T(8,128)(2,1)S(1)}, bf16[32,1024]{1,0:T(8,128)(2,1)S(1)}, u32[]{:S(2)}, u32[]{:S(2)}) collective-permute-start(bf16[32,1024]{1,0:T(8,128)(2,1)S(1)} %get-tuple-element.16), channel_id=1, source_target_pairs={{0,8},{4,12},{8,0},{12,4},{16,24},{20,28},{24,16},{28,20},{1,9},{5... | collective-permute-start | bytes 196616 | tf_op jit(solution)/shard_map/ppermute | solution.py:227
  28.2 5.2 %collective-permute-start.14 = (bf16[32,1024]{1,0:T(8,128)(2,1)S(1)}, bf16[32,1024]{1,0:T(8,128)(2,1)S(1)}, u32[]{:S(2)}, u32[]{:S(2)}) collective-permute-start(bf16[32,1024]{1,0:T(8,128)(2,1)S(1)} %get-tuple-element.17), channel_id=1, source_target_pairs={{0,12},{4,8},{8,4},{12,0},{16,28},{20,24},{24,20},{28,16},{1,13},{... | collective-permute-start | bytes 196616 | tf_op jit(solution)/shard_map/ppermute | solution.py:227
  33.4 4.9 %collective-permute-start.15 = (bf16[16,1024]{1,0:T(8,128)(2,1)S(1)}, bf16[16,1024]{1,0:T(8,128)(2,1)S(1)}, u32[]{:S(2)}, u32[]{:S(2)}) collective-permute-start(bf16[16,1024]{1,0:T(8,128)(2,1)S(1)} %shard_map.100), channel_id=1, source_target_pairs={{0,16},{4,20},{8,24},{12,28},{16,0},{20,4},{24,8},{28,12},{1,17},{... | collective-permute-start | bytes 98312 | tf_op jit(solution)/shard_map/ppermute | solution.py:224

commit v3 on v2

--- a/solution.py
+++ b/solution.py
@@ -116,20 +116,28 @@
         act[e] = (gate / (1.0 + jnp.exp(-gate)) * up * weight).astype(BF16)
 
 
-def combine_kernel(*refs, owners):
-    slots, out, parts, returned = refs[-2], refs[-1], refs[:owners], refs[owners:-2]
-    groups = 1 + len(returned)
+def spread_rows(slots, values, shifts, groups, owners):
     capacity = slots.shape[0] // groups
     own = lax.axis_index("ep") // owners
+    starts = [pl.multiple_of((own + d) % groups * capacity, capacity) for d in shifts]
+    spread = jnp.concatenate([slots[pl.ds(start, capacity), :] for start in starts], axis=0)
+    return lax.dot_general(spread, values, (((0,), (0,)), ((), ())), preferred_element_type=F32)
+
+
+def place_kernel(*refs, owners, groups):
+    slots, out, parts = refs[-2], refs[-1], refs[:owners]
+    capacity = slots.shape[0] // groups
     total = parts[0][:capacity, :].astype(F32)
     for part in parts[1:]:
         total += part[:capacity, :].astype(F32)
-    values = jnp.concatenate([total.astype(BF16)] + [part[...] for part in returned], axis=0)
-    starts = [pl.multiple_of((own + d) % groups * capacity, capacity) for d in range(groups)]
-    spread = jnp.concatenate([slots[pl.ds(start, capacity), :] for start in starts], axis=0)
-    out[...] = lax.dot_general(
-        spread, values, (((0,), (0,)), ((), ())), preferred_element_type=F32
-    ).astype(BF16)
+    out[...] = spread_rows(slots, total.astype(BF16), (0,), groups, owners)
+
+
+def combine_kernel(*refs, owners, groups):
+    returned, placed, slots, out = refs[:-3], refs[-3], refs[-2], refs[-1]
+    values = jnp.concatenate([part[...] for part in returned], axis=0)
+    rows = spread_rows(slots, values, tuple(range(1, groups)), groups, owners)
+    out[...] = (placed[...] + rows).astype(BF16)
 
 
 def down_sum(acts, w_down, steps, total=None):
@@ -298,10 +306,16 @@
         gathered,
     )
     returned = [shift_group(totals[d - 1], -d) for d in range(1, groups)]
+    placed = kernel_call(
+        functools.partial(place_kernel, owners=owners, groups=groups),
+        shape((tokens, out_cols), F32),
+        (*gathered, slots),
+        flops=10**8,
+    )
     return kernel_call(
-        functools.partial(combine_kernel, owners=owners),
+        functools.partial(combine_kernel, owners=owners, groups=groups),
         jax.ShapeDtypeStruct((tokens, out_cols), BF16),
-        (*gathered, *returned, slots),
+        (*returned, placed, slots),
     )
 
 

time: 39.3 us -> 39.3 us (level)
    pallas_call x11 -> x12, Pallas kernels: 4.98 us -> 5.16 us  [kernel_call(): pl.pallas_call(body, out_shape=out_shape, in_specs=[pl.BlockSpec(memory_s...]
  transfers between devices with their start and end apart: 16 -> 16, of which waited for: 11 -> 11; matrix products, arithmetic and copies ran while one was open for 0% -> 0% of each run, Pallas kernels for 4% -> 5%
where the time goes in v3:
time: 39.3 us; the launch traced here: 39.1 us
  starting transfers between devices  19.8 us (50%)
  waiting for transfers between devices  14 us (36%)
  Pallas kernels  5.16 us (13%)
    ppermute x9, starting transfers between devices, to_owner(): return lax.ppermute(value, 'ep', [(s, s ^ j) for s in range(ep_count)])  11.1 us
    ppermute x2, starting transfers between devices, shift_group(): return lax.ppermute(value, 'ep', pairs)  7 us
    ppermute x9, waiting for transfers between devices, to_owner(): return lax.ppermute(value, 'ep', [(s, s ^ j) for s in range(ep_count)])  6.9 us
    pallas_call x12, Pallas kernels, kernel_call(): pl.pallas_call(body, out_shape=out_shape, in_specs=[pl.BlockSpec(memory_s...  5.16 us
    ppermute x1, waiting for transfers between devices, on_device(): lax.ppermute(act, 'tp', [(t, (t + 2 * d) % tp_count) for t in range(tp_co...  4.02 us
    ppermute x2, waiting for transfers between devices, shift_group(): return lax.ppermute(value, 'ep', pairs)  1.81 us
    ppermute x1, starting transfers between devices, on_device(): lax.ppermute(act, 'tp', [(t, (t + 2 * d) % tp_count) for t in range(tp_co...  1.58 us
    ppermute x4, waiting for transfers between devices, swap_cores(): return lax.ppermute(value, 'tp', [(t, t ^ 1) for t in range(tp_count)])  1.28 us
  transfers between devices with their start and end apart: 16, of which 11 were waited for; matrix products, arithmetic and copies ran while one was open for 0% of the time, Pallas kernels for 5%

profile of v3, /device:TPU:0, one launch (start us, length us, event | category | flops | bytes accessed | tf_op | source)
XLA Modules:
  0.0 39.1 jit_solution(6941714380961520079)
XLA Ops:
  0.0 0.0 copy-start.1
  0.0 0.0 copy-start.2
  0.0 1.5 %shard_map.91 = (bf16[16,2176]{1,0:T(8,128)(2,1)S(1)}, bf16[16,2176]{1,0:T(8,128)(2,1)S(1)}, bf16[32,32]{1,0:T(8,128)(2,1)S(1)}) custom-call(bf16[32,4096]{1,0:T(8,128)(2,1)} %refs_0_.1, f32[1,4096]{1,0:T(1,128)} %bitcast.5, s32[1,32]{1,0:T(1,128)} %bitcast.8, s32[4,32]{1,0:T(4,128)} %bitcast.6, f32[1,32]{1,0:T(1,128)} %bitcast.9, f32[4,32]{1,0:T(4,128)} %bitcast.7), custom_call_target="tpu_custom_call" | custom-call | flops 10000000000 | tf_op jit(solution)/shard_map/pallas_call | solution.py:186
  1.5 4.1 %collective-permute-start.3 = (bf16[16,2176]{1,0:T(8,128)(2,1)S(1)}, bf16[16,2176]{1,0:T(8,128)(2,1)S(1)}, u32[]{:S(2)}, u32[]{:S(2)}) collective-permute-start(bf16[16,2176]{1,0:T(8,128)(2,1)S(1)} %get-tuple-element.13), channel_id=1, source_target_pairs={{0,16},{4,20},{8,24},{12,28},{16,0},{20,4},{24,8},{28,12},{1,17},{... | collective-permute-start | bytes 208904 | tf_op jit(solution)/shard_map/ppermute | solution.py:232
  5.6 2.5 %collective-permute-start.2 = (bf16[16,2176]{1,0:T(8,128)(2,1)S(1)}, bf16[16,2176]{1,0:T(8,128)(2,1)S(1)}, u32[]{:S(2)}, u32[]{:S(2)}) collective-permute-start(bf16[16,2176]{1,0:T(8,128)(2,1)S(1)} %get-tuple-element.12.refs_0_), channel_id=1, source_target_pairs={{0,12},{4,8},{8,4},{12,0},{16,28},{20,24},{24,20},{28,16},{1,13},{... | collective-permute-start | bytes 208904 | tf_op jit(solution)/shard_map/ppermute | solution.py:235
  8.1 0.4 %collective-permute-start.1 = (bf16[16,2176]{1,0:T(8,128)(2,1)S(1)}, bf16[16,2176]{1,0:T(8,128)(2,1)S(1)}, u32[]{:S(2)}, u32[]{:S(2)}) collective-permute-start(bf16[16,2176]{1,0:T(8,128)(2,1)S(1)} %get-tuple-element.12.refs_0_), channel_id=1, source_target_pairs={{0,8},{4,12},{8,0},{12,4},{16,24},{20,28},{24,16},{28,20},{1,9},{5... | collective-permute-start | bytes 208904 | tf_op jit(solution)/shard_map/ppermute | solution.py:235
  8.6 0.5 %collective-permute-start = (bf16[16,2176]{1,0:T(8,128)(2,1)S(1)}, bf16[16,2176]{1,0:T(8,128)(2,1)S(1)}, u32[]{:S(2)}, u32[]{:S(2)}) collective-permute-start(bf16[16,2176]{1,0:T(8,128)(2,1)S(1)} %get-tuple-element.12.refs_0_), channel_id=1, source_target_pairs={{0,4},{4,0},{8,12},{12,8},{16,20},{20,16},{24,28},{28,24},{1,5},{5... | collective-permute-start | bytes 208904 | tf_op jit(solution)/shard_map/ppermute | solution.py:235
  9.1 0.0 collective-permute-done.3.refs_0_
  9.1 2.5 %collective-permute-start.6 = (bf16[16,2176]{1,0:T(8,128)(2,1)S(1)}, bf16[16,2176]{1,0:T(8,128)(2,1)S(1)}, u32[]{:S(2)}, u32[]{:S(2)}) collective-permute-start(bf16[16,2176]{1,0:T(8,128)(2,1)S(1)} %collective-permute-done.3.refs_0_), channel_id=1, source_target_pairs={{0,12},{4,8},{8,4},{12,0},{16,28},{20,24},{24,20},{28,16},{1,13},{... | collective-permute-start | bytes 208904 | tf_op jit(solution)/shard_map/ppermute | solution.py:235
  11.6 0.6 %collective-permute-start.5 = (bf16[16,2176]{1,0:T(8,128)(2,1)S(1)}, bf16[16,2176]{1,0:T(8,128)(2,1)S(1)}, u32[]{:S(2)}, u32[]{:S(2)}) collective-permute-start(bf16[16,2176]{1,0:T(8,128)(2,1)S(1)} %collective-permute-done.3.refs_0_), channel_id=1, source_target_pairs={{0,8},{4,12},{8,0},{12,4},{16,24},{20,28},{24,16},{28,20},{1,9},{5... | collective-permute-start | bytes 208904 | tf_op jit(solution)/shard_map/ppermute | solution.py:235
  12.2 0.0 collective-permute-done.2.refs_3_
  12.2 1.0 %collective-permute-start.4 = (bf16[16,2176]{1,0:T(8,128)(2,1)S(1)}, bf16[16,2176]{1,0:T(8,128)(2,1)S(1)}, u32[]{:S(2)}, u32[]{:S(2)}) collective-permute-start(bf16[16,2176]{1,0:T(8,128)(2,1)S(1)} %collective-permute-done.3.refs_0_), channel_id=1, source_target_pairs={{0,4},{4,0},{8,12},{12,8},{16,20},{20,16},{24,28},{28,24},{1,5},{5... | collective-permute-start | bytes 208904 | tf_op jit(solution)/shard_map/ppermute | solution.py:235
  13.2 0.0 collective-permute-done.1.refs_2_
  13.2 0.7 %collective-permute-done.refs_1_ = bf16[16,2176]{1,0:T(8,128)(2,1)S(1)} collective-permute-done((bf16[16,2176]{1,0:T(8,128)(2,1)S(1)}, bf16[16,2176]{1,0:T(8,128)(2,1)S(1)}, u32[]{:S(2)}, u32[]{:S(2)}) %collective-permute-start) | collective-permute-done | bytes 69664 | tf_op jit(solution)/shard_map/ppermute | solution.py:235
  13.9 0.1 collective-permute-start.7
  14.0 0.7 %collective-permute-done.6.refs_3_ = bf16[16,2176]{1,0:T(8,128)(2,1)S(1)} collective-permute-done((bf16[16,2176]{1,0:T(8,128)(2,1)S(1)}, bf16[16,2176]{1,0:T(8,128)(2,1)S(1)}, u32[]{:S(2)}, u32[]{:S(2)}) %collective-permute-start.6) | collective-permute-done | bytes 69664 | tf_op jit(solution)/shard_map/ppermute | solution.py:235
  14.7 1.2 %collective-permute-done.5.refs_2_ = bf16[16,2176]{1,0:T(8,128)(2,1)S(1)} collective-permute-done((bf16[16,2176]{1,0:T(8,128)(2,1)S(1)}, bf16[16,2176]{1,0:T(8,128)(2,1)S(1)}, u32[]{:S(2)}, u32[]{:S(2)}) %collective-permute-start.5) | collective-permute-done | bytes 69664 | tf_op jit(solution)/shard_map/ppermute | solution.py:235
  15.9 0.6 %collective-permute-done.4.refs_1_ = bf16[16,2176]{1,0:T(8,128)(2,1)S(1)} collective-permute-done((bf16[16,2176]{1,0:T(8,128)(2,1)S(1)}, bf16[16,2176]{1,0:T(8,128)(2,1)S(1)}, u32[]{:S(2)}, u32[]{:S(2)}) %collective-permute-start.4) | collective-permute-done | bytes 69664 | tf_op jit(solution)/shard_map/ppermute | solution.py:235
  16.5 0.1 collective-permute-start.8
  16.7 0.0 copy-done.1
  16.7 0.0 copy-done.2
  16.7 0.7 %shard_map.95.partial = f32[2,2,128,256]{3,2,1,0:T(8,128)S(1)} custom-call(bf16[128,2176]{1,0:T(8,128)(2,1)S(1)} %shard_map.94.rows, bf16[2,4096,256]{2,1,0:T(8,128)(2,1)S(1)} %copy-done.1, bf16[2,4096,256]{2,1,0:T(8,128)(2,1)S(1)} %copy-done.2), custom_call_target="tpu_custom_call" | custom-call | flops 536870912 | tf_op jit(solution)/shard_map/pallas_call | solution.py:186
  17.4 0.0 copy-start
  17.4 0.0 collective-permute-done.7.near
  17.4 0.7 %collective-permute-done.8.far = bf16[64,2176]{1,0:T(8,128)(2,1)S(1)} collective-permute-done((bf16[64,2176]{1,0:T(8,128)(2,1)S(1)}, bf16[64,2176]{1,0:T(8,128)(2,1)S(1)}, u32[]{:S(2)}, u32[]{:S(2)}) %collective-permute-start.8) | collective-permute-done | bytes 278560 | tf_op jit(solution)/shard_map/ppermute | solution.py:238
  18.2 0.7 %shard_map.96.refs_0_ = bf16[2,128,256]{2,1,0:T(8,128)(2,1)S(1)} custom-call(bf16[128,2176]{1,0:T(8,128)(2,1)S(1)} %shard_map.94.rows, bf16[64,2176]{1,0:T(8,128)(2,1)S(1)} %collective-permute-done.7.near, bf16[64,2176]{1,0:T(8,128)(2,1)S(1)} %collective-permute-done.8.far, f32[2,2,128,256]{3,2,1,0:T(8,128)S(1)} %shard_map.95.partial, ...), custom_call_target="tpu_custom_call" | custom-call | flops 536870912 | tf_op jit(solution)/shard_map/pallas_call | solution.py:186
  18.9 1.6 %collective-permute-start.9 = (bf16[2,128,256]{2,1,0:T(8,128)(2,1)S(1)}, bf16[2,128,256]{2,1,0:T(8,128)(2,1)S(1)}, u32[]{:S(2)}, u32[]{:S(2)}) collective-permute-start(bf16[2,128,256]{2,1,0:T(8,128)(2,1)S(1)} %shard_map.96.refs_0_), channel_id=1, source_target_pairs={{0,2},{1,3},{2,0},{3,1},{4,6},{5,7},{6,4},{7,5},{8,10},{9,11},{10,... | collective-permute-start | bytes 393224 | tf_op jit(solution)/shard_map/ppermute | solution.py:272
  20.5 0.0 collective-permute-start.11
  20.5 4.0 %collective-permute-done.9.refs_0_ = bf16[2,128,256]{2,1,0:T(8,128)(2,1)S(1)} collective-permute-done((bf16[2,128,256]{2,1,0:T(8,128)(2,1)S(1)}, bf16[2,128,256]{2,1,0:T(8,128)(2,1)S(1)}, u32[]{:S(2)}, u32[]{:S(2)}) %collective-permute-start.9) | collective-permute-done | bytes 131104 | tf_op jit(solution)/shard_map/ppermute | solution.py:272
  24.5 0.0 collective-permute-start.10
  24.5 0.0 collective-permute-done.11.refs_1_
  24.5 0.0 copy-done
  24.5 0.5 %shard_map.97.refs_2_ = f32[128,1024]{1,0:T(8,128)S(1)} custom-call(bf16[2,128,256]{2,1,0:T(8,128)(2,1)S(1)} %shard_map.96.refs_0_, bf16[2,128,256]{2,1,0:T(8,128)(2,1)S(1)} %collective-permute-done.11.refs_1_, bf16[2,1024,1024]{2,1,0:T(8,128)(2,1)S(1)} %copy-done), custom_call_target="tpu_custom_call" | custom-call | flops 100000000 | tf_op jit(solution)/shard_map/pallas_call | solution.py:186
  25.0 0.3 shard_map.98.refs_2_
  25.3 0.5 %collective-permute-done.10.refs_0_ = bf16[2,128,256]{2,1,0:T(8,128)(2,1)S(1)} collective-permute-done((bf16[2,128,256]{2,1,0:T(8,128)(2,1)S(1)}, bf16[2,128,256]{2,1,0:T(8,128)(2,1)S(1)}, u32[]{:S(2)}, u32[]{:S(2)}) %collective-permute-start.10) | collective-permute-done | bytes 131104 | tf_op jit(solution)/shard_map/ppermute | solution.py:238
  25.9 0.3 shard_map.99
  26.2 1.0 %collective-permute-start.12 = (bf16[32,1024]{1,0:T(8,128)(2,1)S(1)}, bf16[32,1024]{1,0:T(8,128)(2,1)S(1)}, u32[]{:S(2)}, u32[]{:S(2)}) collective-permute-start(bf16[32,1024]{1,0:T(8,128)(2,1)S(1)} %get-tuple-element.15), channel_id=1, source_target_pairs={{0,4},{4,0},{8,12},{12,8},{16,20},{20,16},{24,28},{28,24},{1,5},{5... | collective-permute-start | bytes 196616 | tf_op jit(solution)/shard_map/ppermute | solution.py:235
  27.2 1.0 %collective-permute-start.13 = (bf16[32,1024]{1,0:T(8,128)(2,1)S(1)}, bf16[32,1024]{1,0:T(8,128)(2,1)S(1)}, u32[]{:S(2)}, u32[]{:S(2)}) collective-permute-start(bf16[32,1024]{1,0:T(8,128)(2,1)S(1)} %get-tuple-element.16), channel_id=1, source_target_pairs={{0,8},{4,12},{8,0},{12,4},{16,24},{20,28},{24,16},{28,20},{1,9},{5... | collective-permute-start | bytes 196616 | tf_op jit(solution)/shard_map/ppermute | solution.py:235
  28.2 1.5 %collective-permute-start.14 = (bf16[32,1024]{1,0:T(8,128)(2,1)S(1)}, bf16[32,1024]{1,0:T(8,128)(2,1)S(1)}, u32[]{:S(2)}, u32[]{:S(2)}) collective-permute-start(bf16[32,1024]{1,0:T(8,128)(2,1)S(1)} %get-tuple-element.17), channel_id=1, source_target_pairs={{0,12},{4,8},{8,4},{12,0},{16,28},{20,24},{24,20},{28,16},{1,13},{... | collective-permute-start | bytes 196616 | tf_op jit(solution)/shard_map/ppermute | solution.py:235
  29.7 0.8 %collective-permute-done.12.refs_1_ = bf16[32,1024]{1,0:T(8,128)(2,1)S(1)} collective-permute-done((bf16[32,1024]{1,0:T(8,128)(2,1)S(1)}, bf16[32,1024]{1,0:T(8,128)(2,1)S(1)}, u32[]{:S(2)}, u32[]{:S(2)}) %collective-permute-start.12) | collective-permute-done | bytes 65568 | tf_op jit(solution)/shard_map/ppermute | solution.py:235
  30.5 1.1 %collective-permute-done.13.refs_2_ = bf16[32,1024]{1,0:T(8,128)(2,1)S(1)} collective-permute-done((bf16[32,1024]{1,0:T(8,128)(2,1)S(1)}, bf16[32,1024]{1,0:T(8,128)(2,1)S(1)}, u32[]{:S(2)}, u32[]{:S(2)}) %collective-permute-start.13) | collective-permute-done | bytes 65568 | tf_op jit(solution)/shard_map/ppermute | solution.py:235
  31.6 1.8 %collective-permute-done.14.refs_3_ = bf16[32,1024]{1,0:T(8,128)(2,1)S(1)} collective-permute-done((bf16[32,1024]{1,0:T(8,128)(2,1)S(1)}, bf16[32,1024]{1,0:T(8,128)(2,1)S(1)}, u32[]{:S(2)}, u32[]{:S(2)}) %collective-permute-start.14) | collective-permute-done | bytes 65568 | tf_op jit(solution)/shard_map/ppermute | solution.py:235
  33.4 2.9 %collective-permute-start.15 = (bf16[16,1024]{1,0:T(8,128)(2,1)S(1)}, bf16[16,1024]{1,0:T(8,128)(2,1)S(1)}, u32[]{:S(2)}, u32[]{:S(2)}) collective-permute-start(bf16[16,1024]{1,0:T(8,128)(2,1)S(1)} %shard_map.100), channel_id=1, source_target_pairs={{0,16},{4,20},{8,24},{12,28},{16,0},{20,4},{24,8},{28,12},{1,17},{... | collective-permute-start | bytes 98312 | tf_op jit(solution)/shard_map/ppermute | solution.py:232
  36.3 0.2 shard_map.101.refs_1_
  36.5 1.8 %collective-permute-done.15.refs_0_ = bf16[16,1024]{1,0:T(8,128)(2,1)S(1)} collective-permute-done((bf16[16,1024]{1,0:T(8,128)(2,1)S(1)}, bf16[16,1024]{1,0:T(8,128)(2,1)S(1)}, u32[]{:S(2)}, u32[]{:S(2)}) %collective-permute-start.15) | collective-permute-done | bytes 32800 | tf_op jit(solution)/shard_map/ppermute | solution.py:232
  38.3 0.8 %shard_map.102 = bf16[32,1024]{1,0:T(8,128)(2,1)} custom-call(bf16[16,1024]{1,0:T(8,128)(2,1)S(1)} %collective-permute-done.15.refs_0_, f32[32,1024]{1,0:T(8,128)S(1)} %shard_map.101.refs_1_, bf16[32,32]{1,0:T(8,128)(2,1)S(1)} %get-tuple-element.18.refs_4_.refs_2_), custom_call_target="tpu_custom_call" | custom-call | tf_op jit(solution)/shard_map/pallas_call | solution.py:186
  (4 shorter events, 0.1 us)
Async XLA Ops:
  0.0 16.7 %copy-start.1 = (bf16[2,4096,256]{2,1,0:T(8,128)(2,1)S(1)}, bf16[2,4096,256]{2,1,0:T(8,128)(2,1)}, u32[]{:S(2)}) copy-start(bf16[2,4096,256]{2,1,0:T(8,128)(2,1)} %w_gate.3) | copy-start | bytes 12582916
  0.0 16.7 %copy-start.2 = (bf16[2,4096,256]{2,1,0:T(8,128)(2,1)S(1)}, bf16[2,4096,256]{2,1,0:T(8,128)(2,1)}, u32[]{:S(2)}) copy-start(bf16[2,4096,256]{2,1,0:T(8,128)(2,1)} %w_up.3) | copy-start | bytes 12582916
  1.5 7.6 %collective-permute-start.3 = (bf16[16,2176]{1,0:T(8,128)(2,1)S(1)}, bf16[16,2176]{1,0:T(8,128)(2,1)S(1)}, u32[]{:S(2)}, u32[]{:S(2)}) collective-permute-start(bf16[16,2176]{1,0:T(8,128)(2,1)S(1)} %get-tuple-element.13), channel_id=1, source_target_pairs={{0,16},{4,20},{8,24},{12,28},{16,0},{20,4},{24,8},{28,12},{1,17},{... | collective-permute-start | bytes 208904 | tf_op jit(solution)/shard_map/ppermute | solution.py:232
  5.6 6.6 %collective-permute-start.2 = (bf16[16,2176]{1,0:T(8,128)(2,1)S(1)}, bf16[16,2176]{1,0:T(8,128)(2,1)S(1)}, u32[]{:S(2)}, u32[]{:S(2)}) collective-permute-start(bf16[16,2176]{1,0:T(8,128)(2,1)S(1)} %get-tuple-element.12.refs_0_), channel_id=1, source_target_pairs={{0,12},{4,8},{8,4},{12,0},{16,28},{20,24},{24,20},{28,16},{1,13},{... | collective-permute-start | bytes 208904 | tf_op jit(solution)/shard_map/ppermute | solution.py:235
  8.1 5.1 %collective-permute-start.1 = (bf16[16,2176]{1,0:T(8,128)(2,1)S(1)}, bf16[16,2176]{1,0:T(8,128)(2,1)S(1)}, u32[]{:S(2)}, u32[]{:S(2)}) collective-permute-start(bf16[16,2176]{1,0:T(8,128)(2,1)S(1)} %get-tuple-element.12.refs_0_), channel_id=1, source_target_pairs={{0,8},{4,12},{8,0},{12,4},{16,24},{20,28},{24,16},{28,20},{1,9},{5... | collective-permute-start | bytes 208904 | tf_op jit(solution)/shard_map/ppermute | solution.py:235
  8.6 5.3 %collective-permute-start = (bf16[16,2176]{1,0:T(8,128)(2,1)S(1)}, bf16[16,2176]{1,0:T(8,128)(2,1)S(1)}, u32[]{:S(2)}, u32[]{:S(2)}) collective-permute-start(bf16[16,2176]{1,0:T(8,128)(2,1)S(1)} %get-tuple-element.12.refs_0_), channel_id=1, source_target_pairs={{0,4},{4,0},{8,12},{12,8},{16,20},{20,16},{24,28},{28,24},{1,5},{5... | collective-permute-start | bytes 208904 | tf_op jit(solution)/shard_map/ppermute | solution.py:235
  9.1 5.6 %collective-permute-start.6 = (bf16[16,2176]{1,0:T(8,128)(2,1)S(1)}, bf16[16,2176]{1,0:T(8,128)(2,1)S(1)}, u32[]{:S(2)}, u32[]{:S(2)}) collective-permute-start(bf16[16,2176]{1,0:T(8,128)(2,1)S(1)} %collective-permute-done.3.refs_0_), channel_id=1, source_target_pairs={{0,12},{4,8},{8,4},{12,0},{16,28},{20,24},{24,20},{28,16},{1,13},{... | collective-permute-start | bytes 208904 | tf_op jit(solution)/shard_map/ppermute | solution.py:235
  11.6 4.3 %collective-permute-start.5 = (bf16[16,2176]{1,0:T(8,128)(2,1)S(1)}, bf16[16,2176]{1,0:T(8,128)(2,1)S(1)}, u32[]{:S(2)}, u32[]{:S(2)}) collective-permute-start(bf16[16,2176]{1,0:T(8,128)(2,1)S(1)} %collective-permute-done.3.refs_0_), channel_id=1, source_target_pairs={{0,8},{4,12},{8,0},{12,4},{16,24},{20,28},{24,16},{28,20},{1,9},{5... | collective-permute-start | bytes 208904 | tf_op jit(solution)/shard_map/ppermute | solution.py:235
  12.2 4.3 %collective-permute-start.4 = (bf16[16,2176]{1,0:T(8,128)(2,1)S(1)}, bf16[16,2176]{1,0:T(8,128)(2,1)S(1)}, u32[]{:S(2)}, u32[]{:S(2)}) collective-permute-start(bf16[16,2176]{1,0:T(8,128)(2,1)S(1)} %collective-permute-done.3.refs_0_), channel_id=1, source_target_pairs={{0,4},{4,0},{8,12},{12,8},{16,20},{20,16},{24,28},{28,24},{1,5},{5... | collective-permute-start | bytes 208904 | tf_op jit(solution)/shard_map/ppermute | solution.py:235
  13.9 3.5 %collective-permute-start.7 = (bf16[64,2176]{1,0:T(8,128)(2,1)S(1)}, bf16[64,2176]{1,0:T(8,128)(2,1)S(1)}, u32[]{:S(2)}, u32[]{:S(2)}) collective-permute-start(bf16[64,2176]{1,0:T(8,128)(2,1)S(1)} %shard_map.92.refs_0_), channel_id=1, source_target_pairs={{0,1},{1,0},{2,3},{3,2},{4,5},{5,4},{6,7},{7,6},{8,9},{9,8},{10,11... | collective-permute-start | bytes 835592 | tf_op jit(solution)/shard_map/ppermute | solution.py:238
  16.5 1.6 %collective-permute-start.8 = (bf16[64,2176]{1,0:T(8,128)(2,1)S(1)}, bf16[64,2176]{1,0:T(8,128)(2,1)S(1)}, u32[]{:S(2)}, u32[]{:S(2)}) collective-permute-start(bf16[64,2176]{1,0:T(8,128)(2,1)S(1)} %shard_map.93.refs_1_), channel_id=1, source_target_pairs={{0,1},{1,0},{2,3},{3,2},{4,5},{5,4},{6,7},{7,6},{8,9},{9,8},{10,11... | collective-permute-start | bytes 835592 | tf_op jit(solution)/shard_map/ppermute | solution.py:238
  17.4 7.1 %copy-start = (bf16[2,1024,1024]{2,1,0:T(8,128)(2,1)S(1)}, bf16[2,1024,1024]{2,1,0:T(8,128)(2,1)}, u32[]{:S(2)}) copy-start(bf16[2,1024,1024]{2,1,0:T(8,128)(2,1)} %refs_1_.3) | copy-start | bytes 12582916
  18.9 5.6 %collective-permute-start.9 = (bf16[2,128,256]{2,1,0:T(8,128)(2,1)S(1)}, bf16[2,128,256]{2,1,0:T(8,128)(2,1)S(1)}, u32[]{:S(2)}, u32[]{:S(2)}) collective-permute-start(bf16[2,128,256]{2,1,0:T(8,128)(2,1)S(1)} %shard_map.96.refs_0_), channel_id=1, source_target_pairs={{0,2},{1,3},{2,0},{3,1},{4,6},{5,7},{6,4},{7,5},{8,10},{9,11},{10,... | collective-permute-start | bytes 393224 | tf_op jit(solution)/shard_map/ppermute | solution.py:272
  20.5 4.0 %collective-permute-start.11 = (bf16[2,128,256]{2,1,0:T(8,128)(2,1)S(1)}, bf16[2,128,256]{2,1,0:T(8,128)(2,1)S(1)}, u32[]{:S(2)}, u32[]{:S(2)}) collective-permute-start(bf16[2,128,256]{2,1,0:T(8,128)(2,1)S(1)} %shard_map.96.refs_0_), channel_id=1, source_target_pairs={{0,1},{1,0},{2,3},{3,2},{4,5},{5,4},{6,7},{7,6},{8,9},{9,8},{10,11... | collective-permute-start | bytes 393224 | tf_op jit(solution)/shard_map/ppermute | solution.py:238
  24.5 1.3 %collective-permute-start.10 = (bf16[2,128,256]{2,1,0:T(8,128)(2,1)S(1)}, bf16[2,128,256]{2,1,0:T(8,128)(2,1)S(1)}, u32[]{:S(2)}, u32[]{:S(2)}) collective-permute-start(bf16[2,128,256]{2,1,0:T(8,128)(2,1)S(1)} %collective-permute-done.9.refs_0_), channel_id=1, source_target_pairs={{0,1},{1,0},{2,3},{3,2},{4,5},{5,4},{6,7},{7,6},{8,9},{9,8},{10,11... | collective-permute-start | bytes 393224 | tf_op jit(solution)/shard_map/ppermute | solution.py:238
  26.2 4.3 %collective-permute-start.12 = (bf16[32,1024]{1,0:T(8,128)(2,1)S(1)}, bf16[32,1024]{1,0:T(8,128)(2,1)S(1)}, u32[]{:S(2)}, u32[]{:S(2)}) collective-permute-start(bf16[32,1024]{1,0:T(8,128)(2,1)S(1)} %get-tuple-element.15), channel_id=1, source_target_pairs={{0,4},{4,0},{8,12},{12,8},{16,20},{20,16},{24,28},{28,24},{1,5},{5... | collective-permute-start | bytes 196616 | tf_op jit(solution)/shard_map/ppermute | solution.py:235
  27.2 4.4 %collective-permute-start.13 = (bf16[32,1024]{1,0:T(8,128)(2,1)S(1)}, bf16[32,1024]{1,0:T(8,128)(2,1)S(1)}, u32[]{:S(2)}, u32[]{:S(2)}) collective-permute-start(bf16[32,1024]{1,0:T(8,128)(2,1)S(1)} %get-tuple-element.16), channel_id=1, source_target_pairs={{0,8},{4,12},{8,0},{12,4},{16,24},{20,28},{24,16},{28,20},{1,9},{5... | collective-permute-start | bytes 196616 | tf_op jit(solution)/shard_map/ppermute | solution.py:235
  28.2 5.2 %collective-permute-start.14 = (bf16[32,1024]{1,0:T(8,128)(2,1)S(1)}, bf16[32,1024]{1,0:T(8,128)(2,1)S(1)}, u32[]{:S(2)}, u32[]{:S(2)}) collective-permute-start(bf16[32,1024]{1,0:T(8,128)(2,1)S(1)} %get-tuple-element.17), channel_id=1, source_target_pairs={{0,12},{4,8},{8,4},{12,0},{16,28},{20,24},{24,20},{28,16},{1,13},{... | collective-permute-start | bytes 196616 | tf_op jit(solution)/shard_map/ppermute | solution.py:235
  33.4 4.9 %collective-permute-start.15 = (bf16[16,1024]{1,0:T(8,128)(2,1)S(1)}, bf16[16,1024]{1,0:T(8,128)(2,1)S(1)}, u32[]{:S(2)}, u32[]{:S(2)}) collective-permute-start(bf16[16,1024]{1,0:T(8,128)(2,1)S(1)} %shard_map.100), channel_id=1, source_target_pairs={{0,16},{4,20},{8,24},{12,28},{16,0},{20,4},{24,8},{28,12},{1,17},{... | collective-permute-start | bytes 98312 | tf_op jit(solution)/shard_map/ppermute | solution.py:232
